TPU v7x, 512 devices: a whole 4x8x8 slice. The times are simulated.
512 devices in a mesh: kv: 64 (over z, y), tp: 8 (over x, core).
Axes of the slice: x: 4, y: 8, z: 8, core: 2. Of those that a mesh axis runs over, the one named last changes fastest.
Arguments:
- tokens: bfloat16 [128, 4096], P(None, 'kv'), may hold values from -16 to 16
- mix_gain: bfloat16 [4096], P('kv'), may hold values from 0.099609375 to 1.8984375
- ffn_gain: bfloat16 [4096], P('kv'), may hold values from 0.099609375 to 1.8984375
- w_query: bfloat16 [4096, 2048], P('kv', 'tp'), may hold values from -0.09375 to 0.09375
- w_key: bfloat16 [4096, 2048], P('kv', 'tp'), may hold values from -0.09375 to 0.09375
- w_value: bfloat16 [4096, 4096], P('kv', 'tp'), may hold values from -0.09375 to 0.09375
- w_gate: bfloat16 [4096, 4096], P('kv', 'tp'), may hold values from -0.09375 to 0.09375
- w_decay: bfloat16 [4096, 2048], P('kv', 'tp'), may hold values from -0.375 to 0.375
- decay_bias: float32 [2048], P('tp'), may hold values from -7 to 4
- head_gain: bfloat16 [512], replicated, may hold values from 0.099609375 to 1.8984375
- w_output: bfloat16 [4096, 4096], P('tp', 'kv'), may hold values from -0.09375 to 0.09375
- w_ffgate: bfloat16 [4096, 11008], P('kv', 'tp'), may hold values from -0.09375 to 0.09375
- w_ffup: bfloat16 [4096, 11008], P('kv', 'tp'), may hold values from -0.09375 to 0.09375
- w_down: bfloat16 [11008, 4096], P('tp', 'kv'), may hold values from -0.0546875 to 0.0546875
- state: float32 [128, 8, 256, 512], P('kv', 'tp'), may hold values from -6 to 6
Outputs:
- mixed: bfloat16 [128, 4096], P(None, 'kv')
- new_state: float32 [128, 8, 256, 512], P('kv', 'tp')
All inputs are finite; a program needn't handle non-finite values.
Results may differ from a plain program's by a relative error of at most 0.015.
Values may be sent and summed in bfloat16 or wider, within the bound.
No kernel may reach another device: no remote copies, remote signals or barrier semaphores. Data moves between devices by JAX's collectives and lax.ppermute only.
A program may use at most 64 MiB of HBM per device.

v0:
```python
import jax
import jax.numpy as jnp
from jax import lax
from jax.sharding import PartitionSpec as P

epsilon = 1e-06


def split_up(x, dim, devices):
    before, after = (x.shape[:dim], x.shape[dim + 1 :])
    return jnp.moveaxis(x.reshape(*before, devices, -1, *after), dim, 0)


def summed_on_arrival(x, axis, dim):
    devices = lax.axis_size(axis)
    blocks = lax.all_to_all(split_up(x, dim, devices), axis, 0, 0, tiled=True)
    return jnp.sum(blocks.astype(jnp.float32), axis=0)


def in_one_piece(arrays, axis, dim, along):
    columns = [a.reshape(*a.shape[:along], -1) for a in arrays]
    both = jnp.concatenate(columns, axis=along)
    filled, at, gathered = (summed_on_arrival(both, axis, dim), 0, [])
    for a, column in zip(arrays, columns):
        section = filled[..., at : at + column.shape[along]]
        gathered.append(section.reshape(*section.shape[:along], *a.shape[along:]))
        at += column.shape[along]
    return tuple(gathered)


def joined_along(blocks, dim):
    shape = list(blocks.shape[1:])
    shape[dim] *= blocks.shape[0]
    return jnp.moveaxis(blocks, 0, dim).reshape(shape)


def sent_to_all(x, axis):
    devices = lax.axis_size(axis)
    return lax.all_to_all(jnp.broadcast_to(x[None], (devices, *x.shape)), axis, 0, 0, tiled=True)


def collect(x, axis, dim):
    return joined_along(sent_to_all(x, axis), dim)


def over_copies(x, axis):
    everything = sent_to_all(x, axis)
    return jnp.sum(everything.astype(jnp.float32), axis=0)


def local(
    tokens,
    mix_gain,
    ffn_gain,
    w_query,
    w_key,
    w_value,
    w_gate,
    w_decay,
    decay_bias,
    head_gain,
    w_output,
    w_ffgate,
    w_ffup,
    w_down,
    state,
):
    own_rows = state.shape[0]
    local_heads = state.shape[1]
    key_dim = state.shape[2]
    val_dim = state.shape[3]
    model_width = tokens.shape[1] * lax.axis_size("kv")
    token_f32 = tokens.astype(jnp.float32)
    row_squares = jnp.sum(token_f32 * token_f32, axis=1)
    mix_in = (token_f32 * mix_gain.astype(jnp.float32)).astype(jnp.bfloat16)
    query_part = jnp.dot(mix_in, w_query, preferred_element_type=jnp.float32)
    key_part = jnp.dot(mix_in, w_key, preferred_element_type=jnp.float32)
    value_part = jnp.dot(mix_in, w_value, preferred_element_type=jnp.float32)
    gate_part = jnp.dot(mix_in, w_gate, preferred_element_type=jnp.float32)
    decay_part = jnp.dot(mix_in, w_decay, preferred_element_type=jnp.float32)
    query_sum, key_sum, value_sum, gate_sum, decay_sum, own_squares = in_one_piece(
        (
            query_part.astype(jnp.bfloat16),
            key_part.astype(jnp.bfloat16),
            value_part.astype(jnp.bfloat16),
            gate_part.astype(jnp.bfloat16),
            decay_part.astype(jnp.bfloat16),
            row_squares.astype(jnp.bfloat16),
        ),
        "kv",
        0,
        1,
    )
    mix_rms = lax.rsqrt(own_squares / model_width + epsilon)[:, None]
    queries = (query_sum * mix_rms).reshape(own_rows, local_heads, key_dim) * key_dim ** (-0.5)
    key_rows = (key_sum * mix_rms).reshape(own_rows, local_heads, key_dim)
    value_rows = (value_sum * mix_rms).reshape(own_rows, local_heads, val_dim)
    gate_rows = (gate_sum * mix_rms).reshape(own_rows, local_heads, val_dim)
    decay_rows = (decay_sum * mix_rms + decay_bias).reshape(own_rows, local_heads, key_dim)
    log_decay = jax.nn.log_sigmoid(decay_rows) / 16.0
    new_state = (
        jnp.exp(log_decay)[..., None] * state + key_rows[..., :, None] * value_rows[..., None, :]
    )
    attended = jnp.einsum("bhk,bhkv->bhv", queries, new_state, precision=lax.Precision.HIGHEST)
    attended = attended * lax.rsqrt(
        jnp.sum(attended * attended, axis=2, keepdims=True) / val_dim + epsilon
    )
    head_out = (
        (attended * head_gain.astype(jnp.float32) * jax.nn.silu(gate_rows))
        .reshape(own_rows, local_heads * val_dim)
        .astype(jnp.bfloat16)
    )
    head_partial = jnp.dot(collect(head_out, "kv", 0), w_output, preferred_element_type=jnp.float32)
    attn_out = over_copies(head_partial.astype(jnp.bfloat16), "tp").astype(jnp.float32)
    residual_mid = (token_f32 + attn_out).astype(jnp.bfloat16)
    mid_f32 = residual_mid.astype(jnp.float32)
    mid_squares = jnp.sum(mid_f32 * mid_f32, axis=1)
    ffn_in = (mid_f32 * ffn_gain.astype(jnp.float32)).astype(jnp.bfloat16)
    ffgate_part = jnp.dot(ffn_in, w_ffgate, preferred_element_type=jnp.float32)
    ffup_part = jnp.dot(ffn_in, w_ffup, preferred_element_type=jnp.float32)
    ffgate_sum, ffup_sum, square_sum = in_one_piece(
        (
            ffgate_part.astype(jnp.bfloat16),
            ffup_part.astype(jnp.bfloat16),
            mid_squares.astype(jnp.bfloat16),
        ),
        "kv",
        0,
        1,
    )
    ffn_rms = lax.rsqrt(square_sum / model_width + epsilon)[:, None]
    hidden = (jax.nn.silu(ffgate_sum * ffn_rms) * (ffup_sum * ffn_rms)).astype(jnp.bfloat16)
    down_part = jnp.dot(collect(hidden, "kv", 0), w_down, preferred_element_type=jnp.float32)
    ffn_out = over_copies(down_part.astype(jnp.bfloat16), "tp").astype(jnp.float32)
    mixed = (mid_f32 + ffn_out).astype(jnp.bfloat16)
    return (mixed, new_state)


def solution(mesh):
    in_specs = (
        P(None, "kv"),
        P("kv"),
        P("kv"),
        P("kv", "tp"),
        P("kv", "tp"),
        P("kv", "tp"),
        P("kv", "tp"),
        P("kv", "tp"),
        P("tp"),
        P(),
        P("tp", "kv"),
        P("kv", "tp"),
        P("kv", "tp"),
        P("tp", "kv"),
        P("kv", "tp", None, None),
    )
    out_specs = (P(None, "kv"), P("kv", "tp", None, None))
    return jax.shard_map(local, mesh=mesh, in_specs=in_specs, out_specs=out_specs, check_vma=False)
```

profile of v0, /device:TPU:1, one launch (start us, length us, event | category | flops | bytes accessed | tf_op | source)
XLA Modules:
  0.0 142.9 jit_solution(15754888790524407089)
XLA Ops:
  0.7 0.7 convert_element_type.103
  1.4 0.7 fusion.3
  2.1 0.2 convert_element_type.130
  2.3 1.0 convolution_convert_fusion.5
  3.4 1.0 convolution_convert_fusion.4
  4.5 1.0 convolution_convert_fusion.6
  5.6 1.1 convolution_convert_fusion.3
  6.8 0.3 convolution_convert_fusion.2
  7.2 0.7 constant_dynamic-update-slice_fusion.5
  7.9 0.7 constant_dynamic-update-slice_fusion.4
  8.5 0.7 constant_dynamic-update-slice_fusion.3
  9.3 0.7 constant_dynamic-update-slice_fusion.2
  10.0 0.7 constant_dynamic-update-slice_fusion.1
  10.7 0.6 constant_dynamic-update-slice_fusion
  11.4 17.1 %all-to-all-start = ((bf16[64,2,1793]{2,1,0:T(2,128)(2,1)}), bf16[64,2,1793]{2,1,0:T(2,128)(2,1)S(1)}, u32[]{:S(2)}, u32[]{:S(2)}) async-start(bf16[64,2,1793]{2,1,0:T(2,128)(2,1)} %constant_dynamic-update-slice_fusion), calls=%async_computation | async-start | bytes 983040 | tf_op jit(solution)/shard_map/all_to_all | solution.py:16
  28.5 16.7 %all-to-all-done = bf16[64,2,1793]{2,1,0:T(2,128)(2,1)S(1)} async-done(((bf16[64,2,1793]{2,1,0:T(2,128)(2,1)}), bf16[64,2,1793]{2,1,0:T(2,128)(2,1)S(1)}, u32[]{:S(2)}, u32[]{:S(2)}) %all-to-all-start) | async-done | bytes 459040 | tf_op jit(solution)/shard_map/all_to_all | solution.py:16
  45.3 0.4 convert_reduce_fusion.1
  45.7 0.1 fusion.28
  45.8 0.1 slice_multiply_fusion.3
  45.9 0.1 fusion.22
  46.0 0.2 multiply_add_fusion
  46.2 0.6 fusion
  46.8 0.1 fusion.13
  47.0 0.1 fusion.15
  47.1 0.1 broadcast_in_dim.8
  47.2 17.8 %all_to_all.30 = bf16[64,2,512]{2,1,0:T(2,128)(2,1)S(1)} all-to-all(bf16[64,2,512]{2,1,0:T(2,128)(2,1)S(1)} %broadcast_in_dim.8), channel_id=1, replica_groups=mesh['kv'=64,'tp'=8] {'kv'}, dimensions={0} | all-to-all | bytes 262144 | tf_op jit(solution)/shard_map/all_to_all | solution.py:39
  65.1 0.2 convolution_convert_fusion.7
  65.2 0.7 broadcast_in_dim.9
  65.9 7.2 %all-to-all-start.2 = ((bf16[8,128,64]{1,2,0:T(8,128)(2,1)}), bf16[8,128,64]{1,2,0:T(8,128)(2,1)S(1)}, u32[]{:S(2)}, u32[]{:S(2)}) async-start(bf16[8,128,64]{1,2,0:T(8,128)(2,1)} %broadcast_in_dim.9), calls=%async_computation.2 | async-start | bytes 262144 | tf_op jit(solution)/shard_map/all_to_all | solution.py:39
  73.1 5.2 %all-to-all-done.2 = bf16[8,128,64]{1,2,0:T(8,128)(2,1)S(1)} async-done(((bf16[8,128,64]{1,2,0:T(8,128)(2,1)}), bf16[8,128,64]{1,2,0:T(8,128)(2,1)S(1)}, u32[]{:S(2)}, u32[]{:S(2)}) %all-to-all-start.2) | async-done | bytes 131104 | tf_op jit(solution)/shard_map/all_to_all | solution.py:39
  78.4 0.2 convert_element_type.131
  78.6 0.3 convolution_convert_fusion
  79.0 0.2 copy.42
  79.2 0.1 concatenate.29
  79.3 0.3 convolution_convert_fusion.1
  79.7 0.2 copy.41
  79.9 0.1 concatenate.28
  80.0 3.4 %concatenate.30 = bf16[64,2,2753]{2,1,0:T(2,128)(2,1)S(1)} concatenate(bf16[64,2,1376]{2,1,0:T(2,128)(2,1)S(1)} %concatenate.28, bf16[64,2,1376]{2,1,0:T(2,128)(2,1)S(1)} %concatenate.29, bf16[64,2,1]{2,1,0:T(2,128)(2,1)S(1)} %convert_element_type.131), dimensions={2} | concatenate | bytes 1409536 | tf_op jit(solution)/shard_map/concatenate | solution.py:22
  83.4 24.6 %all_to_all.31 = bf16[64,2,2753]{2,1,0:T(2,128)(2,1)S(1)} all-to-all(bf16[64,2,2753]{2,1,0:T(2,128)(2,1)S(1)} %concatenate.30), channel_id=1, replica_groups=mesh['kv'=64,'tp'=8] {'kv'}, dimensions={0} | all-to-all | bytes 1409536 | tf_op jit(solution)/shard_map/all_to_all | solution.py:16
  108.0 0.6 convert_reduce_fusion
  108.6 0.2 fusion.29
  108.8 0.1 fusion.9
  108.9 0.2 broadcast_in_dim.10
  109.1 20.8 %all_to_all.32 = bf16[64,2,1376]{2,1,0:T(2,128)(2,1)S(1)} all-to-all(bf16[64,2,1376]{2,1,0:T(2,128)(2,1)S(1)} %broadcast_in_dim.10), channel_id=1, replica_groups=mesh['kv'=64,'tp'=8] {'kv'}, dimensions={0} | all-to-all | bytes 704512 | tf_op jit(solution)/shard_map/all_to_all | solution.py:39
  130.0 0.3 reshape.123
  130.2 0.2 convolution_convert_fusion.8
  130.5 11.7 %all_to_all.33 = bf16[8,128,64]{1,2,0:T(8,128)(2,1)S(1)} all-to-all(bf16[8,128,64]{1,2,0:T(8,128)(2,1)S(1)} %broadcast_in_dim.11), channel_id=1, replica_groups=mesh['kv'=64,'tp'=8] {'tp'}, dimensions={0} | all-to-all | bytes 262144 | tf_op jit(solution)/shard_map/all_to_all | solution.py:39
  142.3 0.6 fusion.7
  (35 shorter events, 0.5 us)
Async XLA Ops:
  0.6 78.0 %copy-start = (bf16[64,1376]{1,0:T(8,128)(2,1)S(1)}, bf16[64,1376]{1,0:T(8,128)(2,1)}, u32[]{:S(2)}) copy-start(bf16[64,1376]{1,0:T(8,128)(2,1)} %param.27) | copy-start | bytes 528388
  0.6 6.2 %copy-start.3 = (bf16[128,64]{0,1:T(8,128)(2,1)S(1)}, bf16[128,64]{0,1:T(8,128)(2,1)}, u32[]{:S(2)}) copy-start(bf16[128,64]{0,1:T(8,128)(2,1)} %param.15) | copy-start | bytes 49156
  0.7 6.2 %copy-start.6 = (bf16[64,512]{1,0:T(8,128)(2,1)S(1)}, bf16[64,512]{1,0:T(8,128)(2,1)}, u32[]{:S(2)}) copy-start(bf16[64,512]{1,0:T(8,128)(2,1)} %param.21) | copy-start | bytes 196612
  7.2 21.3 %copy-start.8 = (bf16[512]{0:T(512)(128)(2,1)S(1)}, bf16[512]{0:T(512)(128)(2,1)}, u32[]{:S(2)}) copy-start(bf16[512]{0:T(512)(128)(2,1)} %param.24) | copy-start | bytes 3076
  8.5 37.3 %copy-start.9 = (f32[256]{0:T(256)S(1)}, f32[256]{0:T(256)}, u32[]{:S(2)}) copy-start(f32[256]{0:T(256)} %param.23) | copy-start | bytes 3076
  9.3 36.7 %copy-start.2 = (f32[2,1,256,512]{3,2,1,0:T(8,128)S(1)}, f32[2,1,256,512]{3,2,1,0:T(8,128)}, u32[]{:S(2)}) copy-start(f32[2,1,256,512]{3,2,1,0:T(8,128)} %param.29) | copy-start | bytes 3145732
  11.4 33.9 %all-to-all-start = ((bf16[64,2,1793]{2,1,0:T(2,128)(2,1)}), bf16[64,2,1793]{2,1,0:T(2,128)(2,1)S(1)}, u32[]{:S(2)}, u32[]{:S(2)}) async-start(bf16[64,2,1793]{2,1,0:T(2,128)(2,1)} %constant_dynamic-update-slice_fusion), calls=%async_computation | async-start | bytes 983040 | tf_op jit(solution)/shard_map/all_to_all | solution.py:16
  46.2 19.7 %copy-start.1 = (f32[2,1,256,512]{3,2,1,0:T(8,128)}, f32[2,1,256,512]{3,2,1,0:T(8,128)S(1)}, u32[]{:S(2)}) copy-start(f32[2,1,256,512]{3,2,1,0:T(8,128)S(1)} %multiply_add_fusion) | copy-start | bytes 3145732
  46.2 18.8 %copy-start.7 = (bf16[512,64]{0,1:T(8,128)(2,1)S(1)}, bf16[512,64]{0,1:T(8,128)(2,1)}, u32[]{:S(2)}) copy-start(bf16[512,64]{0,1:T(8,128)(2,1)} %param.25) | copy-start | bytes 196612
  46.2 26.9 %copy-start.10 = (bf16[64]{0:T(256)(128)(2,1)S(1)}, bf16[64]{0:T(256)(128)(2,1)}, u32[]{:S(2)}) copy-start(bf16[64]{0:T(256)(128)(2,1)} %param.17) | copy-start | bytes 388
  65.9 12.4 %all-to-all-start.2 = ((bf16[8,128,64]{1,2,0:T(8,128)(2,1)}), bf16[8,128,64]{1,2,0:T(8,128)(2,1)S(1)}, u32[]{:S(2)}, u32[]{:S(2)}) async-start(bf16[8,128,64]{1,2,0:T(8,128)(2,1)} %broadcast_in_dim.9), calls=%async_computation.2 | async-start | bytes 262144 | tf_op jit(solution)/shard_map/all_to_all | solution.py:39
  78.4 1.0 copy-start.4
  108.6 21.6 %copy-start.5 = (bf16[1376,64]{0,1:T(8,128)(2,1)S(1)}, bf16[1376,64]{0,1:T(8,128)(2,1)}, u32[]{:S(2)}) copy-start(bf16[1376,64]{0,1:T(8,128)(2,1)} %param.28) | copy-start | bytes 528388
where the time goes:
time: 144 us; the launch traced here: 143 us
  blocking collectives  75 us (52%)
  starting transfers between devices  24.3 us (17%)
  waiting for transfers between devices  22 us (15%)
  local copies, waits for them, and re-layouts  10.3 us (7%)
  matrix products  6.18 us (4%)
  other arithmetic  4.14 us (3%)
    all_to_all x3, blocking collectives, sent_to_all(): lax.all_to_all(jnp.broadcast_to(x[None], (devices, *x.shape)), axis, 0, 0...  50.4 us
    all_to_all x1, blocking collectives, summed_on_arrival(): blocks = lax.all_to_all(split_up(x, dim, devices), axis, 0, 0, tiled=True)  24.6 us
    all_to_all x1, starting transfers between devices, summed_on_arrival(): blocks = lax.all_to_all(split_up(x, dim, devices), axis, 0, 0, tiled=True)  17.1 us
    all_to_all x1, waiting for transfers between devices, summed_on_arrival(): blocks = lax.all_to_all(split_up(x, dim, devices), axis, 0, 0, tiled=True)  16.7 us
    all_to_all x1, starting transfers between devices, sent_to_all(): lax.all_to_all(jnp.broadcast_to(x[None], (devices, *x.shape)), axis, 0, 0...  7.21 us
    all_to_all x1, waiting for transfers between devices, sent_to_all(): lax.all_to_all(jnp.broadcast_to(x[None], (devices, *x.shape)), axis, 0, 0...  5.23 us
    concatenate x9, local copies, waits for them, and re-layouts, in_one_piece(): both = jnp.concatenate(columns, axis=along)  4.54 us
    unnamed x27, local copies, waits for them, and re-layouts  3.58 us
  transfers between devices with their start and end apart: 2, of which 2 were waited for; matrix products, arithmetic and copies ran while one was open for 0% of the time, Pallas kernels for 0%

commit v1 on v0

v1 whole, which is shorter than its diff:
```python
import functools

import jax
import jax.numpy as jnp
from jax import lax
from jax.experimental import pallas as pl
from jax.experimental.pallas import tpu as pltpu
from jax.sharding import PartitionSpec as P

epsilon = 1e-06


def padded(n):
    return -(-n // 128) * 128


def in_vmem(x):
    return pltpu.with_memory_space_constraint(x, pltpu.VMEM)


def project_kernel(tok_ref, gain_ref, wq, wk, wv, wg, wd, out_ref, tok, gain, q, k, v, g, d, sems):
    pairs = ((tok_ref, tok), (gain_ref, gain), (wq, q), (wk, k), (wv, v), (wg, g), (wd, d))
    copies = [pltpu.make_async_copy(a, b, sems.at[i]) for i, (a, b) in enumerate(pairs)]
    for c in copies:
        c.start()
    copies[0].wait()
    copies[1].wait()
    x = tok[...].astype(jnp.float32).T
    mix_in = (x * gain[...].astype(jnp.float32)).astype(jnp.bfloat16)
    squares = jnp.sum(x * x, axis=1, keepdims=True)
    at = 0
    for i, w in enumerate((q, k, v, g, d)):
        copies[2 + i].wait()
        n = w.shape[1]
        part = jnp.dot(mix_in, w[...], preferred_element_type=jnp.float32)
        out_ref[:, at : at + n] = part.astype(jnp.bfloat16)
        at += n
    rest = out_ref.shape[1] - at
    lane = lax.broadcasted_iota(jnp.int32, (x.shape[0], rest), 1)
    out_ref[:, at:] = jnp.where(lane == 0, squares, 0.0).astype(jnp.bfloat16)


def project(tok_t, gain, weights):
    width, rows = tok_t.shape
    total = sum(w.shape[1] for w in weights)
    arrays = (tok_t, gain, *weights)
    return pl.pallas_call(
        project_kernel,
        out_shape=pltpu.VMEM((rows, total + 128), jnp.bfloat16),
        in_specs=[pl.BlockSpec(memory_space=pl.ANY)] * len(arrays),
        out_specs=pl.BlockSpec(memory_space=pltpu.VMEM),
        scratch_shapes=[pltpu.VMEM(a.shape, a.dtype) for a in arrays]
        + [pltpu.SemaphoreType.DMA((len(arrays),))],
        name="project",
    )(*arrays)


def widen_kernel(parts, tok_ref, gain_ref, wg, wu, out_ref, mid_ref):
    mid = (tok_ref[...].astype(jnp.float32) + jnp.sum(parts[...].astype(jnp.float32), axis=0)).astype(
        jnp.bfloat16
    )
    mid_ref[...] = mid
    x = mid.astype(jnp.float32).T
    ffn_in = (x * gain_ref[...].astype(jnp.float32)).astype(jnp.bfloat16)
    squares = jnp.sum(x * x, axis=1, keepdims=True)
    n = wg.shape[1]
    m = out_ref.shape[1] // 2
    gate = jnp.dot(ffn_in, wg[...], preferred_element_type=jnp.float32)
    up = jnp.dot(ffn_in, wu[...], preferred_element_type=jnp.float32)
    lane = lax.broadcasted_iota(jnp.int32, (x.shape[0], m - n), 1)
    out_ref[:, :n] = gate.astype(jnp.bfloat16)
    out_ref[:, n:m] = jnp.where(lane == 0, squares, 0.0).astype(jnp.bfloat16)
    out_ref[:, m : m + n] = up.astype(jnp.bfloat16)
    out_ref[:, m + n :] = jnp.zeros((x.shape[0], m - n), jnp.bfloat16)


def widen(parts, tok_t, gain, wg, wu):
    width, rows = tok_t.shape
    return pl.pallas_call(
        widen_kernel,
        out_shape=(
            pltpu.VMEM((rows, 2 * padded(wg.shape[1] + 1)), jnp.bfloat16),
            pltpu.VMEM(tok_t.shape, jnp.bfloat16),
        ),
        in_specs=[pl.BlockSpec(memory_space=pltpu.VMEM)] * 5,
        out_specs=[pl.BlockSpec(memory_space=pltpu.VMEM)] * 2,
        name="widen",
    )(*(in_vmem(a) for a in (parts, tok_t, gain, wg, wu)))


def exchanged(blocks, axis):
    return lax.all_to_all(blocks, axis, 0, 0, tiled=True)


def summed(blocks):
    return jnp.sum(blocks.astype(jnp.float32), axis=0)


def to_all(x, axis):
    return exchanged(jnp.broadcast_to(x[None], (lax.axis_size(axis), *x.shape)), axis)


def local(
    tokens,
    mix_gain,
    ffn_gain,
    w_query,
    w_key,
    w_value,
    w_gate,
    w_decay,
    decay_bias,
    head_gain,
    w_output,
    w_ffgate,
    w_ffup,
    w_down,
    state,
):
    own_rows, heads, key_dim, val_dim = state.shape
    kv = lax.axis_size("kv")
    model_width = tokens.shape[1] * kv
    tok_t = tokens.T
    made = project(tok_t, mix_gain[None, :], (w_query, w_key, w_value, w_gate, w_decay))
    arrived, head_gain = lax.optimization_barrier(
        (exchanged(made.reshape(kv, own_rows, -1), "kv"), head_gain)
    )
    sums = summed(arrived)
    kd, vd = heads * key_dim, heads * val_dim
    ends = (kd, 2 * kd, 2 * kd + vd, 2 * kd + 2 * vd, 3 * kd + 2 * vd)
    query_sum, key_sum, value_sum, gate_sum, decay_sum = (
        sums[:, a:b] for a, b in zip((0,) + ends[:-1], ends)
    )
    mix_rms = lax.rsqrt(sums[:, ends[-1] : ends[-1] + 1] / model_width + epsilon)
    queries = (query_sum * mix_rms).reshape(own_rows, heads, key_dim) * key_dim ** (-0.5)
    key_rows = (key_sum * mix_rms).reshape(own_rows, heads, key_dim)
    value_rows = (value_sum * mix_rms).reshape(own_rows, heads, val_dim)
    gate_rows = (gate_sum * mix_rms).reshape(own_rows, heads, val_dim)
    decay_rows = (decay_sum * mix_rms + decay_bias).reshape(own_rows, heads, key_dim)
    log_decay = jax.nn.log_sigmoid(decay_rows) / 16.0
    new_state = (
        jnp.exp(log_decay)[..., None] * state + key_rows[..., :, None] * value_rows[..., None, :]
    )
    attended = jnp.einsum("bhk,bhkv->bhv", queries, new_state, precision=lax.Precision.HIGHEST)
    attended = attended * lax.rsqrt(
        jnp.sum(attended * attended, axis=2, keepdims=True) / val_dim + epsilon
    )
    head_out = (
        (attended * head_gain.astype(jnp.float32) * jax.nn.silu(gate_rows))
        .reshape(own_rows, vd)
        .astype(jnp.bfloat16)
    )
    heads_all = to_all(head_out, "kv").reshape(-1, vd)
    attn_part = lax.dot_general(
        w_output, heads_all, (((0,), (1,)), ((), ())), preferred_element_type=jnp.float32
    ).astype(jnp.bfloat16)
    attn_parts = to_all(attn_part, "tp")
    wide, mid_t = widen(attn_parts, tok_t, ffn_gain[None, :], w_ffgate, w_ffup)
    sums = summed(exchanged(wide.reshape(kv, own_rows, -1), "kv"))
    units = w_ffgate.shape[1]
    half = wide.shape[1] // 2
    ffn_rms = lax.rsqrt(sums[:, units : units + 1] / model_width + epsilon)
    hidden = (
        jax.nn.silu(sums[:, :units] * ffn_rms) * (sums[:, half : half + units] * ffn_rms)
    ).astype(jnp.bfloat16)
    hidden_all = to_all(hidden, "kv").reshape(-1, units)
    down_part = lax.dot_general(
        w_down, hidden_all, (((0,), (1,)), ((), ())), preferred_element_type=jnp.float32
    ).astype(jnp.bfloat16)
    mixed = (mid_t.astype(jnp.float32) + summed(to_all(down_part, "tp"))).astype(jnp.bfloat16)
    return (mixed.T, new_state)


def solution(mesh):
    in_specs = (
        P(None, "kv"),
        P("kv"),
        P("kv"),
        P("kv", "tp"),
        P("kv", "tp"),
        P("kv", "tp"),
        P("kv", "tp"),
        P("kv", "tp"),
        P("tp"),
        P(),
        P("tp", "kv"),
        P("kv", "tp"),
        P("kv", "tp"),
        P("tp", "kv"),
        P("kv", "tp", None, None),
    )
    out_specs = (P(None, "kv"), P("kv", "tp", None, None))
    return jax.shard_map(local, mesh=mesh, in_specs=in_specs, out_specs=out_specs, check_vma=False)
```

time: 144 us -> 129 us (0.90)
  blocking collectives: 75 us -> 121 us
  starting transfers between devices: 24.3 us -> 0 us
  waiting for transfers between devices: 22 us -> 0 us
  local copies, waits for them, and re-layouts: 10.3 us -> 1.15 us
  matrix products: 6.18 us -> 1.02 us
  Pallas kernels: 0 us -> 2.2 us
  other arithmetic: 4.14 us -> 2.64 us
    all_to_all x4 -> x6, blocking collectives: 75 us -> 121 us  [exchanged(): return lax.all_to_all(blocks, axis, 0, 0, tiled=True)]
    all_to_all x2 -> x0, starting transfers between devices: 24.3 us -> none  [the longest x1 17.1 us: summed_on_arrival(): blocks = lax.all_to_all(split_up(x, dim, devices), axis, 0, 0, tiled=True)]
    all_to_all x2 -> x0, waiting for transfers between devices: 22 us -> none  [the longest x1 16.7 us: summed_on_arrival(): blocks = lax.all_to_all(split_up(x, dim, devices), axis, 0, 0, tiled=True)]
    dot_general x9 -> x2, matrix products: 5.58 us -> 0.42 us  [the longest x1 0.26 us: local(): lax.dot_general(w_down, hidden_all, (((0,), (1,)), ((), ())), preferred_e...]
    concatenate x9 -> x0, local copies, waits for them, and re-layouts: 4.54 us -> none  [in_one_piece(): both = jnp.concatenate(columns, axis=along)]
    unnamed x27 -> x20, local copies, waits for them, and re-layouts: 3.58 us -> 0.07 us
    pallas_call x0 -> x2, Pallas kernels: none -> 2.2 us  [the longest x1 1.79 us: project(): pl.pallas_call(project_kernel, out_shape=pltpu.VMEM((rows, total + 128),...]
  transfers between devices with their start and end apart: 2 -> 0, of which waited for: 2 -> 0; matrix products, arithmetic and copies ran while one was open for 0% -> 0% of each run, Pallas kernels for 0% -> 0%
where the time goes in v1:
time: 129 us
  blocking collectives  121 us (94%)
  other arithmetic  2.64 us (2%)
  Pallas kernels  2.2 us (2%)
    all_to_all x6, blocking collectives, exchanged(): return lax.all_to_all(blocks, axis, 0, 0, tiled=True)  121 us

profile of v1, /device:TPU:1, one launch (start us, length us, event | category | flops | bytes accessed | tf_op | source)
XLA Modules:
  0.0 129.0 jit_solution(17808557098418956045)
XLA Ops:
  0.6 0.0 copy-start
  0.6 1.8 %project.1 = bf16[128,1920]{1,0:T(8,128)(2,1)S(1)} custom-call(bf16[64,128]{1,0:T(8,128)(2,1)} %bitcast.29, bf16[1,64]{1,0:T(2,128)(2,1)} %bitcast.32, bf16[64,256]{1,0:T(8,128)(2,1)} %wq.1, bf16[64,256]{1,0:T(8,128)(2,1)} %wk.1, bf16[64,512]{1,0:T(8,128)(2,1)} %wv.1, bf16[64,512]{1,0:T(8,128)(2,1)} %wg.2, bf16[64,256]{1,0:T(8,128)(2,1)} %wd.1), custom_call_target="tpu_custom_call" | custom-call | tf_op jit(solution)/shard_map/project/pallas_call | solution.py:47
  2.4 0.0 copy-start.8
  2.5 0.0 copy-start.9
  2.5 0.0 copy-start.6
  2.5 0.2 reshape.86
  2.7 33.8 %all_to_all.30 = bf16[64,2,1920]{2,1,0:T(2,128)(2,1)S(1)} all-to-all(bf16[64,2,1920]{2,1,0:T(2,128)(2,1)S(1)} %reshape.86), channel_id=1, replica_groups=mesh['kv'=64,'tp'=8] {'kv'}, dimensions={0} | all-to-all | bytes 983040 | tf_op jit(solution)/shard_map/all_to_all | solution.py:92
  36.5 0.4 convert_reduce_fusion.1
  36.9 0.1 fusion.23
  37.0 0.0 copy-done.8
  37.0 0.1 slice_multiply_fusion.3
  37.1 0.0 copy-done.9
  37.1 0.1 fusion.17
  37.2 0.0 copy-done.6
  37.2 0.2 multiply_add_fusion
  37.4 0.0 copy-start.5
  37.5 0.0 copy-start.7
  37.5 0.0 copy-start.1
  37.5 0.0 copy-start.2
  37.5 0.0 copy-start.3
  37.5 0.0 copy-start.4
  37.5 0.6 fusion.2
  38.1 0.1 fusion.8
  38.3 0.1 fusion.10
  38.4 0.1 broadcast_in_dim.13
  38.4 17.8 %all_to_all.31 = bf16[64,2,512]{2,1,0:T(2,128)(2,1)S(1)} all-to-all(bf16[64,2,512]{2,1,0:T(2,128)(2,1)S(1)} %broadcast_in_dim.13), channel_id=1, replica_groups=mesh['kv'=64,'tp'=8] {'kv'}, dimensions={0} | all-to-all | bytes 262144 | tf_op jit(solution)/shard_map/all_to_all | solution.py:92
  56.3 0.1 reshape.88
  56.3 0.0 copy-done.7
  56.3 0.2 fusion
  56.5 12.3 %all_to_all.32.parts = bf16[8,64,128]{2,1,0:T(8,128)(2,1)S(1)} all-to-all(bf16[8,64,128]{2,1,0:T(8,128)(2,1)S(1)} %broadcast_in_dim.14), channel_id=1, replica_groups=mesh['kv'=64,'tp'=8] {'tp'}, dimensions={0} | all-to-all | bytes 262144 | tf_op jit(solution)/shard_map/all_to_all | solution.py:92
  68.8 0.0 copy-done.5
  68.8 0.0 copy-done.1
  68.8 0.0 copy-done.2
  68.8 0.0 copy-done.3
  68.8 0.0 copy-done.4
  68.8 0.4 widen.1
  69.2 0.3 reshape.89
  69.5 24.6 %all_to_all.33 = bf16[64,2,2816]{2,1,0:T(2,128)(2,1)S(1)} all-to-all(bf16[64,2,2816]{2,1,0:T(2,128)(2,1)S(1)} %reshape.89), channel_id=1, replica_groups=mesh['kv'=64,'tp'=8] {'kv'}, dimensions={0} | all-to-all | bytes 1441792 | tf_op jit(solution)/shard_map/all_to_all | solution.py:92
  94.1 0.6 convert_reduce_fusion
  94.7 0.2 fusion.24
  94.9 0.1 fusion.6
  95.0 0.2 broadcast_in_dim.16
  95.2 20.8 %all_to_all.34 = bf16[64,2,1376]{2,1,0:T(2,128)(2,1)S(1)} all-to-all(bf16[64,2,1376]{2,1,0:T(2,128)(2,1)S(1)} %broadcast_in_dim.16), channel_id=1, replica_groups=mesh['kv'=64,'tp'=8] {'kv'}, dimensions={0} | all-to-all | bytes 704512 | tf_op jit(solution)/shard_map/all_to_all | solution.py:92
  116.0 0.3 reshape.90
  116.3 0.0 copy-done
  116.3 0.3 fusion.1
  116.6 11.7 %all_to_all.35 = bf16[8,64,128]{2,1,0:T(8,128)(2,1)S(1)} all-to-all(bf16[8,64,128]{2,1,0:T(8,128)(2,1)S(1)} %broadcast_in_dim.17), channel_id=1, replica_groups=mesh['kv'=64,'tp'=8] {'tp'}, dimensions={0} | all-to-all | bytes 262144 | tf_op jit(solution)/shard_map/all_to_all | solution.py:92
  128.4 0.6 fusion.4
  (5 shorter events, 0.1 us)
Async XLA Ops:
  0.6 115.7 %copy-start = (bf16[1376,64]{0,1:T(8,128)(2,1)S(1)}, bf16[1376,64]{0,1:T(8,128)(2,1)}, u32[]{:S(2)}) copy-start(bf16[1376,64]{0,1:T(8,128)(2,1)} %param.28) | copy-start | bytes 528388
  2.4 34.6 %copy-start.8 = (bf16[512]{0:T(512)(128)(2,1)S(1)}, bf16[512]{0:T(512)(128)(2,1)}, u32[]{:S(2)}) copy-start(bf16[512]{0:T(512)(128)(2,1)} %param.24) | copy-start | bytes 3076
  2.5 34.7 %copy-start.9 = (f32[256]{0:T(256)S(1)}, f32[256]{0:T(256)}, u32[]{:S(2)}) copy-start(f32[256]{0:T(256)} %param.23) | copy-start | bytes 3076
  2.5 34.7 %copy-start.6 = (f32[2,1,256,512]{3,2,1,0:T(8,128)S(1)}, f32[2,1,256,512]{3,2,1,0:T(8,128)}, u32[]{:S(2)}) copy-start(f32[2,1,256,512]{3,2,1,0:T(8,128)} %param.29) | copy-start | bytes 3145732
  37.4 31.4 %copy-start.5 = (f32[2,1,256,512]{3,2,1,0:T(8,128)}, f32[2,1,256,512]{3,2,1,0:T(8,128)S(1)}, u32[]{:S(2)}) copy-start(f32[2,1,256,512]{3,2,1,0:T(8,128)S(1)} %multiply_add_fusion) | copy-start | bytes 3145732
  37.5 18.9 %copy-start.7 = (bf16[512,64]{0,1:T(8,128)(2,1)S(1)}, bf16[512,64]{0,1:T(8,128)(2,1)}, u32[]{:S(2)}) copy-start(bf16[512,64]{0,1:T(8,128)(2,1)} %param.25) | copy-start | bytes 196612
  37.5 31.3 %copy-start.1 = (bf16[64,1376]{1,0:T(8,128)(2,1)S(1)}, bf16[64,1376]{1,0:T(8,128)(2,1)}, u32[]{:S(2)}) copy-start(bf16[64,1376]{1,0:T(8,128)(2,1)} %wg.3) | copy-start | bytes 528388
  37.5 31.3 %copy-start.2 = (bf16[64,1376]{1,0:T(8,128)(2,1)S(1)}, bf16[64,1376]{1,0:T(8,128)(2,1)}, u32[]{:S(2)}) copy-start(bf16[64,1376]{1,0:T(8,128)(2,1)} %wu.1) | copy-start | bytes 528388
  37.5 31.3 %copy-start.3 = (bf16[128,64]{0,1:T(8,128)(2,1)S(1)}, bf16[128,64]{0,1:T(8,128)(2,1)}, u32[]{:S(2)}) copy-start(bf16[128,64]{0,1:T(8,128)(2,1)} %param.15) | copy-start | bytes 49156
  37.5 31.3 %copy-start.4 = (bf16[64]{0:T(256)(128)(2,1)S(1)}, bf16[64]{0:T(256)(128)(2,1)}, u32[]{:S(2)}) copy-start(bf16[64]{0:T(256)(128)(2,1)} %param.17) | copy-start | bytes 388

commit v2 on v1

v2 whole, which is shorter than its diff:
```python
import functools

import jax
import jax.numpy as jnp
from jax import lax
from jax.experimental import pallas as pl
from jax.experimental.pallas import tpu as pltpu
from jax.sharding import Mesh
from jax.sharding import PartitionSpec as P

epsilon = 1e-06
KV = ("z", "h", "r")
LINE = ("z", "h")


def padded(n):
    return -(-n // 128) * 128


def in_vmem(x):
    return pltpu.with_memory_space_constraint(x, pltpu.VMEM)


def whole(count):
    return [pl.BlockSpec(memory_space=pltpu.VMEM)] * count


def cut_of(units):
    return units // 256 * 128


def half_of(units):
    return padded(units - cut_of(units) + 1)


def project_kernel(*refs, count):
    sources, outs = (refs[:count], refs[count : count + 3])
    held, sems = (refs[count + 3 : -1], refs[-1])
    copies = [pltpu.make_async_copy(a, b, sems.at[i]) for i, (a, b) in enumerate(zip(sources, held))]
    for c in copies:
        c.start()
    out_ref, mine_ref, sent_ref = outs
    tok, gain, ffn_gain = held[:3]
    weights, splits = (held[3:-3], held[-3:])
    copies[0].wait()
    copies[1].wait()
    x = tok[...].astype(jnp.float32).T
    mix_in = (x * gain[...].astype(jnp.float32)).astype(jnp.bfloat16)
    squares = jnp.sum(x * x, axis=1, keepdims=True)
    at = 0
    for i, w in enumerate(weights):
        copies[3 + i].wait()
        n = w.shape[1]
        part = jnp.dot(mix_in, w[...], preferred_element_type=jnp.float32)
        out_ref[:, at : at + n] = part.astype(jnp.bfloat16)
        at += n
    rest = out_ref.shape[1] - at
    lane = lax.broadcasted_iota(jnp.int32, (x.shape[0], rest), 1)
    out_ref[:, at:] = jnp.where(lane == 0, squares, 0.0).astype(jnp.bfloat16)
    copies[2].wait()
    for c in copies[3 + len(weights) :]:
        c.wait()
    rows, units = splits[0].shape
    cut, half = (cut_of(units), half_of(units))

    def fill(ref, member, first):
        a, b = ((0, cut), (cut, units))[member]
        for i, w in enumerate(splits):
            ref[:, i * half : i * half + b - a] = w[:, a:b]
            ref[:, i * half + b - a : (i + 1) * half] = jnp.zeros((rows, half - (b - a)), w.dtype)
        seqs = tok.shape[1]
        end = len(splits) * half
        ref[:, end : end + seqs] = tok[...]
        ref[:, end + seqs :] = jnp.zeros((rows, 2 * rows), ref.dtype)
        side = 0 if first else rows
        ref[0:1, end + seqs + side : end + seqs + side + rows] = ffn_gain[...]

    for member in range(2):

        @pl.when(lax.axis_index("r") == member)
        def _():
            fill(mine_ref, member, True)
            fill(sent_ref, 1 - member, False)


def project(tok_t, gain, ffn_gain, weights, splits):
    width, rows = tok_t.shape
    total = sum(w.shape[1] for w in weights)
    pack = len(splits) * half_of(splits[0].shape[1]) + rows + 2 * width
    arrays = (tok_t, gain, ffn_gain, *weights, *splits)
    return pl.pallas_call(
        functools.partial(project_kernel, count=len(arrays)),
        out_shape=(
            pltpu.VMEM((rows, total + 128), jnp.bfloat16),
            pltpu.VMEM((width, pack), jnp.bfloat16),
            pltpu.VMEM((width, pack), jnp.bfloat16),
        ),
        in_specs=[pl.BlockSpec(memory_space=pl.ANY)] * len(arrays),
        out_specs=whole(3),
        scratch_shapes=[pltpu.VMEM(a.shape, a.dtype) for a in arrays]
        + [pltpu.SemaphoreType.DMA((len(arrays),))],
        name="project",
    )(*arrays)


def widen_kernel(parts, mine, got, out_ref, mid_ref):
    r = lax.axis_index("r")
    _, seqs = mid_ref.shape
    half = out_ref.shape[1] // 2
    end = 3 * half

    def mid_of(ref, at):
        total = jnp.sum(parts[at].astype(jnp.float32), axis=0)
        return (ref[:, end : end + seqs].astype(jnp.float32) + total).astype(jnp.bfloat16)

    own = mid_of(mine, r)
    mid_ref[...] = own
    x = jnp.concatenate([own, mid_of(got, 1 - r)], axis=0).astype(jnp.float32).T
    gains = mine[0:1, end + seqs :].astype(jnp.float32) + got[0:1, end + seqs :].astype(jnp.float32)
    ffn_in = (x * gains).astype(jnp.bfloat16)
    squares = jnp.sum(x * x, axis=1, keepdims=True)
    weights = jnp.concatenate([mine[:, : 2 * half], got[:, : 2 * half]], axis=0)
    made = jnp.dot(ffn_in, weights, preferred_element_type=jnp.float32)
    lane = lax.broadcasted_iota(jnp.int32, (seqs, 128), 1)
    out_ref[...] = made.astype(jnp.bfloat16)
    out_ref[:, half - 128 : half] = jnp.where(lane == 127, squares, made[:, half - 128 : half]).astype(
        jnp.bfloat16
    )


def widen(parts, mine, got, half):
    width, seqs = parts.shape[2:]
    return pl.pallas_call(
        widen_kernel,
        out_shape=(
            pltpu.VMEM((seqs, 2 * half), jnp.bfloat16),
            pltpu.VMEM((width, seqs), jnp.bfloat16),
        ),
        in_specs=whole(3),
        out_specs=whole(2),
        name="widen",
    )(*(in_vmem(a) for a in (parts, mine, got)))


def narrow_kernel(hidden, mine, got, out_ref):
    r = lax.axis_index("r")
    half = hidden.shape[1]
    copies, _ = out_ref.shape[1:3]
    for ref, at in ((mine, r), (got, 1 - r)):
        made = lax.dot_general(
            ref[:, 2 * half : 3 * half],
            hidden[...],
            (((1,), (1,)), ((), ())),
            preferred_element_type=jnp.float32,
        ).astype(jnp.bfloat16)
        for j in range(copies):
            out_ref[at, j] = made


def narrow(hidden, mine, got, tp):
    width, seqs = (mine.shape[0], hidden.shape[0])
    return pl.pallas_call(
        narrow_kernel,
        out_shape=pltpu.VMEM((2, tp, width, seqs), jnp.bfloat16),
        in_specs=whole(3),
        out_specs=pl.BlockSpec(memory_space=pltpu.VMEM),
        name="narrow",
    )(*(in_vmem(a) for a in (hidden, mine, got)))


def exchanged(blocks, axis):
    return lax.all_to_all(blocks, axis, 0, 0, tiled=True)


def summed(blocks):
    return jnp.sum(blocks.astype(jnp.float32), axis=0)


def to_all(x, axis):
    return exchanged(jnp.broadcast_to(x[None], (lax.axis_size(axis), *x.shape)), axis)


def local(
    tokens,
    mix_gain,
    ffn_gain,
    w_query,
    w_key,
    w_value,
    w_gate,
    w_decay,
    decay_bias,
    head_gain,
    w_output,
    w_ffgate,
    w_ffup,
    w_down,
    state,
):
    own_rows, heads, key_dim, val_dim = state.shape
    kv, tp, line = (lax.axis_size(a) for a in (KV, "tp", LINE))
    model_width = tokens.shape[1] * kv
    made, mine, sent = project(
        tokens.T,
        mix_gain[None, :],
        ffn_gain[None, :],
        (w_query, w_key, w_value, w_gate, w_decay),
        (w_ffgate, w_ffup, w_down.T),
    )
    got = lax.ppermute(sent, "r", ((0, 1), (1, 0)))
    arrived = exchanged(made.reshape(kv, own_rows, -1), KV)
    arrived, head_gain = lax.optimization_barrier((arrived, head_gain))
    sums = summed(arrived)
    kd, vd = heads * key_dim, heads * val_dim
    ends = (kd, 2 * kd, 2 * kd + vd, 2 * kd + 2 * vd, 3 * kd + 2 * vd)
    query_sum, key_sum, value_sum, gate_sum, decay_sum = (
        sums[:, a:b] for a, b in zip((0,) + ends[:-1], ends)
    )
    mix_rms = lax.rsqrt(sums[:, ends[-1] : ends[-1] + 1] / model_width + epsilon)
    queries = (query_sum * mix_rms).reshape(own_rows, heads, key_dim) * key_dim ** (-0.5)
    key_rows = (key_sum * mix_rms).reshape(own_rows, heads, key_dim)
    value_rows = (value_sum * mix_rms).reshape(own_rows, heads, val_dim)
    gate_rows = (gate_sum * mix_rms).reshape(own_rows, heads, val_dim)
    decay_rows = (decay_sum * mix_rms + decay_bias).reshape(own_rows, heads, key_dim)
    log_decay = jax.nn.log_sigmoid(decay_rows) / 16.0
    new_state = (
        jnp.exp(log_decay)[..., None] * state + key_rows[..., :, None] * value_rows[..., None, :]
    )
    attended = jnp.einsum("bhk,bhkv->bhv", queries, new_state, precision=lax.Precision.HIGHEST)
    attended = attended * lax.rsqrt(
        jnp.sum(attended * attended, axis=2, keepdims=True) / val_dim + epsilon
    )
    head_out = (
        (attended * head_gain.astype(jnp.float32) * jax.nn.silu(gate_rows))
        .reshape(own_rows, vd)
        .astype(jnp.bfloat16)
    )
    heads_all = to_all(head_out, KV).reshape(-1, vd)
    attn_part = lax.dot_general(
        w_output, heads_all, (((0,), (1,)), ((), ())), preferred_element_type=jnp.float32
    ).astype(jnp.bfloat16)
    attn_part, got = lax.optimization_barrier((attn_part, got))
    width, seqs = attn_part.shape
    attn_parts = to_all(attn_part, ("r", "tp")).reshape(2, tp, width, seqs)
    half = half_of(w_ffgate.shape[1])
    wide, mid_t = widen(attn_parts, mine, got, half)
    sums = summed(exchanged(wide.reshape(line, seqs // line, -1), LINE))
    ffn_rms = lax.rsqrt(sums[:, half - 1 : half] / model_width + epsilon)
    gated = jax.nn.silu(sums[:, :half] * ffn_rms) * (sums[:, half:] * ffn_rms)
    hidden = gated.astype(jnp.bfloat16)
    hidden_all = to_all(hidden, LINE).reshape(seqs, half)
    down_parts = narrow(hidden_all, mine, got, tp).reshape(2 * tp, width, seqs)
    mixed = (mid_t.astype(jnp.float32) + summed(exchanged(down_parts, ("r", "tp")))).astype(
        jnp.bfloat16
    )
    return (mixed.T, new_state)


def solution(mesh):
    in_specs = (
        P(None, KV),
        P(KV),
        P(KV),
        P(KV, "tp"),
        P(KV, "tp"),
        P(KV, "tp"),
        P(KV, "tp"),
        P(KV, "tp"),
        P("tp"),
        P(),
        P("tp", KV),
        P(KV, "tp"),
        P(KV, "tp"),
        P("tp", KV),
        P(KV, "tp", None, None),
    )
    out_specs = (P(None, KV), P(KV, "tp", None, None))
    kv, tp = mesh.devices.shape
    lines = Mesh(mesh.devices.reshape(8, kv // 16, 2, tp), (*KV, "tp"))
    return jax.shard_map(local, mesh=lines, in_specs=in_specs, out_specs=out_specs, check_vma=False)
```

time: 129 us -> 131 us (1.016)
  blocking collectives: 121 us -> 104 us
  starting transfers between devices: 0 us -> 9.4 us
  waiting for transfers between devices: 0 us -> 8.63 us
    all_to_all x6 -> x5, blocking collectives: 121 us -> 104 us  [exchanged(): return lax.all_to_all(blocks, axis, 0, 0, tiled=True)]
    all_to_all x0 -> x1, waiting for transfers between devices: none -> 8.62 us  [exchanged(): return lax.all_to_all(blocks, axis, 0, 0, tiled=True)]
    all_to_all x0 -> x1, starting transfers between devices: none -> 6.49 us  [exchanged(): return lax.all_to_all(blocks, axis, 0, 0, tiled=True)]
    ppermute x0 -> x1, starting transfers between devices: none -> 2.92 us  [local(): got = lax.ppermute(sent, 'r', ((0, 1), (1, 0)))]
  transfers between devices with their start and end apart: 0 -> 2, of which waited for: 0 -> 1; matrix products, arithmetic and copies ran while one was open for 0% -> 0% of each run, Pallas kernels for 0% -> 0%
where the time goes in v2:
time: 131 us
  blocking collectives  104 us (79%)
  starting transfers between devices  9.4 us (7%)
  waiting for transfers between devices  8.63 us (7%)
  Pallas kernels  2.52 us (2%)
  local copies, waits for them, and re-layouts  2.39 us (2%)
  other arithmetic  2.23 us (2%)
    all_to_all x5, blocking collectives, exchanged(): return lax.all_to_all(blocks, axis, 0, 0, tiled=True)  104 us
    all_to_all x1, waiting for transfers between devices, exchanged(): return lax.all_to_all(blocks, axis, 0, 0, tiled=True)  8.62 us
    all_to_all x1, starting transfers between devices, exchanged(): return lax.all_to_all(blocks, axis, 0, 0, tiled=True)  6.49 us
    ppermute x1, starting transfers between devices, local(): got = lax.ppermute(sent, 'r', ((0, 1), (1, 0)))  2.92 us
  transfers between devices with their start and end apart: 2, of which 1 were waited for; matrix products, arithmetic and copies ran while one was open for 0% of the time, Pallas kernels for 0%

profile of v2, /device:TPU:1, one launch (start us, length us, event | category | flops | bytes accessed | tf_op | source)
XLA Modules:
  0.0 130.8 jit_solution(5531634124116348639)
XLA Ops:
  0.6 0.0 copy-start
  0.6 1.9 %project.1 = (bf16[128,1920]{1,0:T(8,128)(2,1)S(1)}, bf16[64,2560]{1,0:T(8,128)(2,1)S(1)}, bf16[64,2560]{1,0:T(8,128)(2,1)S(1)}) custom-call(bf16[64,128]{1,0:T(8,128)(2,1)} %bitcast.31, bf16[1,64]{1,0:T(2,128)(2,1)} %bitcast.32, bf16[1,64]{1,0:T(2,128)(2,1)} %bitcast.33, bf16[64,256]{1,0:T(8,128)(2,1)} %refs_3_.1, bf16[64,256]{1,0:T(8,128)(2,1)} %refs_4_.1, ...), custom_call_target="tpu_custom_call" | custom-call | tf_op jit(solution)/shard_map/project/pallas_call | solution.py:91
  2.6 0.2 reshape.91
  2.8 0.0 copy-start.2
  2.8 33.8 %all_to_all.30 = bf16[64,2,1920]{2,1,0:T(2,128)(2,1)S(1)} all-to-all(bf16[64,2,1920]{2,1,0:T(2,128)(2,1)S(1)} %reshape.91), channel_id=1, replica_groups=mesh['z'=8,'h'=4,'r'=2,'tp'=8] {'z','h','r'}, dimensions={0} | all-to-all | bytes 983040 | tf_op jit(solution)/shard_map/all_to_all | solution.py:172
  36.6 0.4 convert_reduce_fusion
  37.0 0.0 copy-start.3
  37.0 0.1 fusion.23
  37.2 0.6 copy-done.3
  37.7 0.0 copy-start.4
  37.7 0.1 slice_multiply_fusion.3
  37.8 0.6 copy-done.4
  38.4 0.1 fusion.19
  38.5 0.0 copy-done.2
  38.5 0.2 multiply_add_fusion
  38.7 0.0 copy-start.1
  38.7 0.6 fusion.1
  39.3 0.1 fusion.7
  39.5 0.1 fusion.9
  39.6 0.7 broadcast_in_dim.12
  40.3 6.5 %all-to-all-start.1 = ((bf16[64,2,512]{2,1,0:T(2,128)(2,1)}), bf16[64,2,512]{2,1,0:T(2,128)(2,1)S(1)}, u32[]{:S(2)}, u32[]{:S(2)}) async-start(bf16[64,2,512]{2,1,0:T(2,128)(2,1)} %broadcast_in_dim.12), calls=%async_computation.1 | async-start | bytes 262144 | tf_op jit(solution)/shard_map/all_to_all | solution.py:172
  46.8 2.9 %collective-permute-start = (bf16[64,2560]{1,0:T(8,128)(2,1)S(1)}, bf16[64,2560]{1,0:T(8,128)(2,1)S(1)}, u32[]{:S(2)}, u32[]{:S(2)}) collective-permute-start(bf16[64,2560]{1,0:T(8,128)(2,1)S(1)} %get-tuple-element.14), channel_id=1, source_target_pairs={{0,8},{8,0},{1,9},{9,1},{2,10},{10,2},{3,11},{11,3},{4,12},{12,4},... | collective-permute-start | bytes 983048 | tf_op jit(solution)/shard_map/ppermute | solution.py:210
  49.7 8.6 %all-to-all-done.1 = bf16[64,2,512]{2,1,0:T(2,128)(2,1)S(1)} async-done(((bf16[64,2,512]{2,1,0:T(2,128)(2,1)}), bf16[64,2,512]{2,1,0:T(2,128)(2,1)S(1)}, u32[]{:S(2)}, u32[]{:S(2)}) %all-to-all-start.1) | async-done | bytes 131104 | tf_op jit(solution)/shard_map/all_to_all | solution.py:172
  58.3 0.1 reshape.93
  58.4 0.0 copy-done
  58.4 0.2 fusion
  58.6 0.0 collective-permute-done.got
  58.6 0.0 copy-done.1
  58.6 14.8 %all_to_all.31 = bf16[16,64,128]{2,1,0:T(8,128)(2,1)S(1)} all-to-all(bf16[16,64,128]{2,1,0:T(8,128)(2,1)S(1)} %broadcast_in_dim.13), channel_id=1, replica_groups=mesh['z'=8,'h'=4,'r'=2,'tp'=8] {'r','tp'}, dimensions={0} | all-to-all | bytes 524288 | tf_op jit(solution)/shard_map/all_to_all | solution.py:172
  73.5 0.3 widen.1
  73.8 0.1 reshape.95
  73.9 22.6 %all_to_all.32 = bf16[32,4,1536]{2,1,0:T(4,128)(2,1)S(1)} all-to-all(bf16[32,4,1536]{2,1,0:T(4,128)(2,1)S(1)} %reshape.95), channel_id=1, replica_groups=mesh['z'=8,'h'=4,'r'=2,'tp'=8] {'z','h'}, dimensions={0} | all-to-all | bytes 786432 | tf_op jit(solution)/shard_map/all_to_all | solution.py:172
  96.5 0.2 convert_reduce_fusion.1
  96.7 0.2 fusion.15
  96.9 0.1 fusion.5
  97.0 0.1 broadcast_in_dim.14
  97.0 19.6 %all_to_all.33 = bf16[32,4,768]{2,1,0:T(4,128)(2,1)S(1)} all-to-all(bf16[32,4,768]{2,1,0:T(4,128)(2,1)S(1)} %broadcast_in_dim.14), channel_id=1, replica_groups=mesh['z'=8,'h'=4,'r'=2,'tp'=8] {'z','h'}, dimensions={0} | all-to-all | bytes 393216 | tf_op jit(solution)/shard_map/all_to_all | solution.py:172
  116.6 0.1 reshape.96.hidden
  116.7 0.3 narrow.1
  116.9 13.2 %all_to_all.34 = bf16[16,64,128]{2,1,0:T(8,128)(2,1)S(1)} all-to-all(bf16[16,64,128]{2,1,0:T(8,128)(2,1)S(1)} %bitcast.29), channel_id=1, replica_groups=mesh['z'=8,'h'=4,'r'=2,'tp'=8] {'r','tp'}, dimensions={0} | all-to-all | bytes 524288 | tf_op jit(solution)/shard_map/all_to_all | solution.py:172
  130.2 0.6 fusion.3
  (4 shorter events, 0.1 us)
Async XLA Ops:
  0.6 57.8 %copy-start = (bf16[512,64]{0,1:T(8,128)(2,1)S(1)}, bf16[512,64]{0,1:T(8,128)(2,1)}, u32[]{:S(2)}) copy-start(bf16[512,64]{0,1:T(8,128)(2,1)} %param.25) | copy-start | bytes 196612
  2.8 35.7 %copy-start.2 = (f32[2,1,256,512]{3,2,1,0:T(8,128)S(1)}, f32[2,1,256,512]{3,2,1,0:T(8,128)}, u32[]{:S(2)}) copy-start(f32[2,1,256,512]{3,2,1,0:T(8,128)} %param.29) | copy-start | bytes 3145732
  37.0 0.7 copy-start.3
  37.7 0.7 copy-start.4
  38.7 19.9 %copy-start.1 = (f32[2,1,256,512]{3,2,1,0:T(8,128)}, f32[2,1,256,512]{3,2,1,0:T(8,128)S(1)}, u32[]{:S(2)}) copy-start(f32[2,1,256,512]{3,2,1,0:T(8,128)S(1)} %multiply_add_fusion) | copy-start | bytes 3145732
  40.3 18.0 %all-to-all-start.1 = ((bf16[64,2,512]{2,1,0:T(2,128)(2,1)}), bf16[64,2,512]{2,1,0:T(2,128)(2,1)S(1)}, u32[]{:S(2)}, u32[]{:S(2)}) async-start(bf16[64,2,512]{2,1,0:T(2,128)(2,1)} %broadcast_in_dim.12), calls=%async_computation.1 | async-start | bytes 262144 | tf_op jit(solution)/shard_map/all_to_all | solution.py:172
  46.8 11.8 %collective-permute-start = (bf16[64,2560]{1,0:T(8,128)(2,1)S(1)}, bf16[64,2560]{1,0:T(8,128)(2,1)S(1)}, u32[]{:S(2)}, u32[]{:S(2)}) collective-permute-start(bf16[64,2560]{1,0:T(8,128)(2,1)S(1)} %get-tuple-element.14), channel_id=1, source_target_pairs={{0,8},{8,0},{1,9},{9,1},{2,10},{10,2},{3,11},{11,3},{4,12},{12,4},... | collective-permute-start | bytes 983048 | tf_op jit(solution)/shard_map/ppermute | solution.py:210

commit v3 on v2

v3 whole, which is shorter than its diff:
```python
import functools

import jax
import jax.numpy as jnp
from jax import lax
from jax.experimental import pallas as pl
from jax.experimental.pallas import tpu as pltpu
from jax.sharding import PartitionSpec as P

epsilon = 1e-06


def member(kv):
    return (kv ^ (kv >> 2)) & 1


def lines(kv):
    return [[i for i in range(kv) if member(i) == m] for m in range(2)]


def pairs(kv, tp):
    return [
        [i * tp + t for i in sorted((j, j + 1), key=member) for t in range(tp)]
        for j in range(0, kv, 2)
    ]


def padded(n):
    return -(-n // 128) * 128


def in_vmem(x):
    return pltpu.with_memory_space_constraint(x, pltpu.VMEM)


def whole(count):
    return [pl.BlockSpec(memory_space=pltpu.VMEM)] * count


def cut_of(units):
    return units // 256 * 128


def half_of(units):
    return padded(units - cut_of(units) + 1)


def project_kernel(*refs, count):
    sources, outs = (refs[:count], refs[count : count + 5])
    held, sems = (refs[count + 5 : -1] + outs[3:], refs[-1])
    copies = [pltpu.make_async_copy(a, b, sems.at[i]) for i, (a, b) in enumerate(zip(sources, held))]
    for c in copies:
        c.start()
    out_ref, mine_ref, sent_ref = outs[:3]
    tok, gain, ffn_gain = held[:3]
    weights, splits = (held[3:-5], held[-5:-2])
    copies[0].wait()
    copies[1].wait()
    x = tok[...].astype(jnp.float32).T
    mix_in = (x * gain[...].astype(jnp.float32)).astype(jnp.bfloat16)
    squares = jnp.sum(x * x, axis=1, keepdims=True)
    at = 0
    for i, w in enumerate(weights):
        copies[3 + i].wait()
        n = w.shape[1]
        part = jnp.dot(mix_in, w[...], preferred_element_type=jnp.float32)
        out_ref[:, at : at + n] = part.astype(jnp.bfloat16)
        at += n
    rest = out_ref.shape[1] - at
    lane = lax.broadcasted_iota(jnp.int32, (x.shape[0], rest), 1)
    out_ref[:, at:] = jnp.where(lane == 0, squares, 0.0).astype(jnp.bfloat16)
    copies[2].wait()
    for c in copies[3 + len(weights) :]:
        c.wait()
    rows, units = splits[0].shape
    cut, half = (cut_of(units), half_of(units))

    def fill(ref, m, first):
        a, b = ((0, cut), (cut, units))[m]
        for i, w in enumerate(splits):
            ref[:, i * half : i * half + b - a] = w[:, a:b]
            ref[:, i * half + b - a : (i + 1) * half] = jnp.zeros((rows, half - (b - a)), w.dtype)
        seqs = tok.shape[1]
        end = len(splits) * half
        ref[:, end : end + seqs] = tok[...]
        ref[:, end + seqs :] = jnp.zeros((rows, 2 * rows), ref.dtype)
        side = 0 if first else rows
        ref[0:1, end + seqs + side : end + seqs + side + rows] = ffn_gain[...]

    for m in range(2):

        @pl.when(member(lax.axis_index("kv")) == m)
        def _():
            fill(mine_ref, m, True)
            fill(sent_ref, 1 - m, False)


def project(tok_t, gain, ffn_gain, weights, splits, kept):
    width, rows = tok_t.shape
    total = sum(w.shape[1] for w in weights)
    pack = len(splits) * half_of(splits[0].shape[1]) + rows + 2 * width
    arrays = (tok_t, gain, ffn_gain, *weights, *splits, *kept)
    return pl.pallas_call(
        functools.partial(project_kernel, count=len(arrays)),
        out_shape=(
            pltpu.VMEM((rows, total + 128), jnp.bfloat16),
            pltpu.VMEM((width, pack), jnp.bfloat16),
            pltpu.VMEM((width, pack), jnp.bfloat16),
            *(pltpu.VMEM(a.shape, a.dtype) for a in kept),
        ),
        in_specs=[pl.BlockSpec(memory_space=pl.ANY)] * len(arrays),
        out_specs=whole(5),
        scratch_shapes=[pltpu.VMEM(a.shape, a.dtype) for a in arrays[:-2]]
        + [pltpu.SemaphoreType.DMA((len(arrays),))],
        name="project",
    )(*arrays)


def attend_kernel(sums, bias, gain, state, key_ref, value_ref, decay_ref, out_ref, *, model_width):
    rows, _, kd, vd = state.shape
    base = sums[...]
    rms = lax.rsqrt(base[:, 3 * kd + 2 * vd : 3 * kd + 2 * vd + 1] / model_width + epsilon)
    q = base[:, :kd] * rms * kd**-0.5
    k = base[:, kd : 2 * kd] * rms
    v = base[:, 2 * kd : 2 * kd + vd] * rms
    g = base[:, 2 * kd + vd : 2 * kd + 2 * vd] * rms
    x = base[:, 2 * kd + 2 * vd : 3 * kd + 2 * vd] * rms + bias[...]
    log_sigmoid = jnp.minimum(x, 0.0) - jnp.log1p(jnp.exp(-jnp.abs(x)))
    decay = jnp.exp(log_sigmoid / 16.0)
    key_ref[...] = k
    value_ref[...] = v
    decay_ref[...] = decay
    fresh = jnp.sum(q * k, axis=1, keepdims=True) * v
    columns = jnp.concatenate([q * decay, jnp.zeros((8 - rows, kd), jnp.float32)], axis=0).T
    step = 32
    found = []
    for s in range(rows):
        total = jnp.zeros((8, vd), jnp.float32)
        for at in range(0, kd, step):
            read = columns[at : at + step, s : s + 1] * state[s, 0, at : at + step]
            total = total + jnp.sum(read.reshape(step // 8, 8, vd), axis=0)
        found.append(jnp.sum(total, axis=0, keepdims=True))
    attended = jnp.concatenate(found, axis=0) + fresh
    scale = lax.rsqrt(jnp.sum(attended * attended, axis=1, keepdims=True) / vd + epsilon)
    gains = jnp.concatenate([gain[i : i + 1] for i in range(gain.shape[0])], axis=1)
    gated = attended * scale * gains.astype(jnp.float32) * (g / (1.0 + jnp.exp(-g)))
    out_ref[...] = gated.astype(jnp.bfloat16)


def attend(sums, bias, gain, state, model_width):
    rows, _, kd, vd = state.shape
    return pl.pallas_call(
        functools.partial(attend_kernel, model_width=model_width),
        out_shape=(
            pltpu.VMEM((rows, kd), jnp.float32),
            pltpu.VMEM((rows, vd), jnp.float32),
            pltpu.VMEM((rows, kd), jnp.float32),
            pltpu.VMEM((rows, vd), jnp.bfloat16),
        ),
        in_specs=whole(4),
        out_specs=whole(4),
        name="attend",
    )(*(in_vmem(a) for a in (sums, bias, gain, state)))


def widen_kernel(parts, mine, got, _, out_ref, mid_ref):
    r = member(lax.axis_index("kv"))
    _, seqs = mid_ref.shape
    half = out_ref.shape[1] // 2
    end = 3 * half

    def mid_of(ref, at):
        total = jnp.sum(parts[at].astype(jnp.float32), axis=0)
        return (ref[:, end : end + seqs].astype(jnp.float32) + total).astype(jnp.bfloat16)

    own = mid_of(mine, r)
    mid_ref[...] = own
    x = jnp.concatenate([own, mid_of(got, 1 - r)], axis=0).astype(jnp.float32).T
    gains = mine[0:1, end + seqs :].astype(jnp.float32) + got[0:1, end + seqs :].astype(jnp.float32)
    ffn_in = (x * gains).astype(jnp.bfloat16)
    squares = jnp.sum(x * x, axis=1, keepdims=True)
    weights = jnp.concatenate([mine[:, : 2 * half], got[:, : 2 * half]], axis=0)
    made = jnp.dot(ffn_in, weights, preferred_element_type=jnp.float32)
    lane = lax.broadcasted_iota(jnp.int32, (seqs, 128), 1)
    out_ref[...] = made.astype(jnp.bfloat16)
    out_ref[:, half - 128 : half] = jnp.where(lane == 127, squares, made[:, half - 128 : half]).astype(
        jnp.bfloat16
    )


def widen(parts, mine, got, new_state, half):
    width, seqs = parts.shape[2:]
    return pl.pallas_call(
        widen_kernel,
        out_shape=(
            pltpu.VMEM((seqs, 2 * half), jnp.bfloat16),
            pltpu.VMEM((width, seqs), jnp.bfloat16),
        ),
        in_specs=whole(4),
        out_specs=whole(2),
        name="widen",
    )(*(in_vmem(a) for a in (parts, mine, got, new_state)))


def narrow_kernel(hidden, mine, got, out_ref):
    r = member(lax.axis_index("kv"))
    half = hidden.shape[1]
    copies, _ = out_ref.shape[1:3]
    for ref, at in ((mine, r), (got, 1 - r)):
        made = lax.dot_general(
            ref[:, 2 * half : 3 * half],
            hidden[...],
            (((1,), (1,)), ((), ())),
            preferred_element_type=jnp.float32,
        ).astype(jnp.bfloat16)
        for j in range(copies):
            out_ref[at, j] = made


def narrow(hidden, mine, got, tp):
    width, seqs = (mine.shape[0], hidden.shape[0])
    return pl.pallas_call(
        narrow_kernel,
        out_shape=pltpu.VMEM((2, tp, width, seqs), jnp.bfloat16),
        in_specs=whole(3),
        out_specs=pl.BlockSpec(memory_space=pltpu.VMEM),
        name="narrow",
    )(*(in_vmem(a) for a in (hidden, mine, got)))


def exchanged(blocks, axis, groups=None):
    return lax.all_to_all(blocks, axis, 0, 0, axis_index_groups=groups, tiled=True)


def summed(blocks):
    return jnp.sum(blocks.astype(jnp.float32), axis=0)


def copies_of(x, count):
    return jnp.broadcast_to(x[None], (count, *x.shape))


def local(
    tokens,
    mix_gain,
    ffn_gain,
    w_query,
    w_key,
    w_value,
    w_gate,
    w_decay,
    decay_bias,
    head_gain,
    w_output,
    w_ffgate,
    w_ffup,
    w_down,
    state,
):
    own_rows, heads, _, val_dim = state.shape
    kv, tp = (lax.axis_size(a) for a in ("kv", "tp"))
    model_width = tokens.shape[1] * kv
    made, mine, sent, bias, head_scale = project(
        tokens.T,
        mix_gain[None, :],
        ffn_gain[None, :],
        (w_query, w_key, w_value, w_gate, w_decay),
        (w_ffgate, w_ffup, w_down.T),
        (decay_bias[None, :], head_gain.reshape(-1, 128)),
    )
    got = lax.ppermute(sent, "kv", [(i, i ^ 1) for i in range(kv)])
    arrived = exchanged(made.reshape(kv, own_rows, -1), "kv")
    keys, values, decay, head_out = attend(summed(arrived), bias, head_scale, state, model_width)
    new_state = (
        decay[:, None, :, None] * state + keys[:, None, :, None] * values[:, None, None, :]
    )
    head_out, new_state = lax.optimization_barrier((head_out, new_state))
    heads_all = exchanged(copies_of(head_out, kv), "kv").reshape(-1, heads * val_dim)
    attn_part = lax.dot_general(
        w_output, heads_all, (((0,), (1,)), ((), ())), preferred_element_type=jnp.float32
    ).astype(jnp.bfloat16)
    attn_part, got = lax.optimization_barrier((attn_part, got))
    width, seqs = attn_part.shape
    pair, line = (pairs(kv, tp), lines(kv))
    attn_parts = exchanged(copies_of(attn_part, 2 * tp), ("kv", "tp"), pair)
    half = half_of(w_ffgate.shape[1])
    wide, mid_t = widen(attn_parts.reshape(2, tp, width, seqs), mine, got, new_state, half)
    count = len(line[0])
    sums = summed(exchanged(wide.reshape(count, seqs // count, -1), "kv", line))
    ffn_rms = lax.rsqrt(sums[:, half - 1 : half] / model_width + epsilon)
    gated = jax.nn.silu(sums[:, :half] * ffn_rms) * (sums[:, half:] * ffn_rms)
    hidden = gated.astype(jnp.bfloat16)
    hidden_all = exchanged(copies_of(hidden, count), "kv", line).reshape(seqs, half)
    down_parts = narrow(hidden_all, mine, got, tp).reshape(2 * tp, width, seqs)
    mixed = (
        mid_t.astype(jnp.float32) + summed(exchanged(down_parts, ("kv", "tp"), pair))
    ).astype(jnp.bfloat16)
    return (mixed.T, new_state)


def solution(mesh):
    in_specs = (
        P(None, "kv"),
        P("kv"),
        P("kv"),
        P("kv", "tp"),
        P("kv", "tp"),
        P("kv", "tp"),
        P("kv", "tp"),
        P("kv", "tp"),
        P("tp"),
        P(),
        P("tp", "kv"),
        P("kv", "tp"),
        P("kv", "tp"),
        P("tp", "kv"),
        P("kv", "tp", None, None),
    )
    out_specs = (P(None, "kv"), P("kv", "tp", None, None))
    return jax.shard_map(local, mesh=mesh, in_specs=in_specs, out_specs=out_specs, check_vma=False)
```

time: 131 us -> 127 us (0.969)
  blocking collectives: 104 us -> 102 us
    all_to_all x5, blocking collectives: 104 us -> 102 us  [exchanged(): lax.all_to_all(blocks, axis, 0, 0, axis_index_groups=groups, tiled=True)]
where the time goes in v3:
time: 127 us
  blocking collectives  102 us (80%)
  starting transfers between devices  9.4 us (7%)
  waiting for transfers between devices  8.63 us (7%)
  Pallas kernels  3.03 us (2%)
  other arithmetic  1.74 us (1%)
  local copies, waits for them, and re-layouts  1.38 us (1%)
    all_to_all x5, blocking collectives, exchanged(): lax.all_to_all(blocks, axis, 0, 0, axis_index_groups=groups, tiled=True)  102 us
    all_to_all x1, waiting for transfers between devices, exchanged(): lax.all_to_all(blocks, axis, 0, 0, axis_index_groups=groups, tiled=True)  8.62 us
    all_to_all x1, starting transfers between devices, exchanged(): lax.all_to_all(blocks, axis, 0, 0, axis_index_groups=groups, tiled=True)  6.49 us
    ppermute x1, starting transfers between devices, local(): got = lax.ppermute(sent, 'kv', [(i, i ^ 1) for i in range(kv)])  2.92 us
  transfers between devices with their start and end apart: 2, of which 1 were waited for; matrix products, arithmetic and copies ran while one was open for 0% of the time, Pallas kernels for 0%

profile of v3, /device:TPU:1, one launch (start us, length us, event | category | flops | bytes accessed | tf_op | source)
XLA Modules:
  0.0 127.1 jit_solution(9707045556097024269)
XLA Ops:
  0.6 0.0 copy-start
  0.7 2.0 %project.1 = (bf16[128,1920]{1,0:T(8,128)(2,1)S(1)}, bf16[64,2560]{1,0:T(8,128)(2,1)S(1)}, bf16[64,2560]{1,0:T(8,128)(2,1)S(1)}, f32[1,256]{1,0:T(1,128)S(1)}, bf16[4,128]{1,0:T(4,128)(2,1)S(1)}) custom-call(bf16[64,128]{1,0:T(8,128)(2,1)} %bitcast.17, bf16[1,64]{1,0:T(2,128)(2,1)} %bitcast.20, bf16[1,64]{1,0:T(2,128)(2,1)} %bitcast.21, ...), custom_call_target="tpu_custom_call" | custom-call | tf_op jit(solution)/shard_map/project/pallas_call | solution.py:103
  2.6 0.0 copy-start.1
  2.6 0.2 reshape.42
  2.8 33.8 %all_to_all.30 = bf16[64,2,1920]{2,1,0:T(2,128)(2,1)S(1)} all-to-all(bf16[64,2,1920]{2,1,0:T(2,128)(2,1)S(1)} %reshape.42), channel_id=1, replica_groups=mesh['kv'=64,'tp'=8] {'kv'}, dimensions={0} | all-to-all | bytes 983040 | tf_op jit(solution)/shard_map/all_to_all | solution.py:232
  36.7 0.4 convert_reduce_fusion.sums
  37.1 0.0 copy-done.1
  37.1 0.5 attend.1
  37.6 0.2 multiply_add_fusion._
  37.8 0.0 copy-start.2
  37.8 0.9 broadcast_in_dim.15
  38.7 6.5 %all-to-all-start.1 = ((bf16[64,2,512]{2,1,0:T(2,128)(2,1)}), bf16[64,2,512]{2,1,0:T(2,128)(2,1)S(1)}, u32[]{:S(2)}, u32[]{:S(2)}) async-start(bf16[64,2,512]{2,1,0:T(2,128)(2,1)} %broadcast_in_dim.15), calls=%async_computation.1 | async-start | bytes 262144 | tf_op jit(solution)/shard_map/all_to_all | solution.py:232
  45.2 2.9 %collective-permute-start = (bf16[64,2560]{1,0:T(8,128)(2,1)S(1)}, bf16[64,2560]{1,0:T(8,128)(2,1)S(1)}, u32[]{:S(2)}, u32[]{:S(2)}) collective-permute-start(bf16[64,2560]{1,0:T(8,128)(2,1)S(1)} %get-tuple-element.25), channel_id=1, source_target_pairs={{0,8},{8,0},{16,24},{24,16},{32,40},{40,32},{48,56},{56,48},{64,72... | collective-permute-start | bytes 983048 | tf_op jit(solution)/shard_map/ppermute | solution.py:271
  48.1 8.6 %all-to-all-done.1 = bf16[64,2,512]{2,1,0:T(2,128)(2,1)S(1)} async-done(((bf16[64,2,512]{2,1,0:T(2,128)(2,1)}), bf16[64,2,512]{2,1,0:T(2,128)(2,1)S(1)}, u32[]{:S(2)}, u32[]{:S(2)}) %all-to-all-start.1) | async-done | bytes 131104 | tf_op jit(solution)/shard_map/all_to_all | solution.py:232
  56.7 0.1 reshape.43
  56.8 0.0 copy-done
  56.8 0.2 fusion
  56.9 0.0 collective-permute-done.got
  57.0 14.9 %all_to_all.31 = bf16[16,64,128]{2,1,0:T(8,128)(2,1)S(1)} all-to-all(bf16[16,64,128]{2,1,0:T(8,128)(2,1)S(1)} %broadcast_in_dim.16), channel_id=1, replica_groups={{0,1,2,3,4,5,6,7,8,9,10,11,12,13,14,15},{16,17,18,19,20,21,22,23,24,25,..., dimensions={0} | all-to-all | bytes 524288 | tf_op jit(solution)/shard_map/all_to_all | solution.py:232
  71.9 0.3 widen.1
  72.2 0.0 copy-done.2
  72.2 0.1 reshape.45
  72.3 21.8 %all_to_all.32 = bf16[32,4,1536]{2,1,0:T(4,128)(2,1)S(1)} all-to-all(bf16[32,4,1536]{2,1,0:T(4,128)(2,1)S(1)} %reshape.45), channel_id=1, replica_groups={{0,16,40,56,64,80,104,120,128,144,168,184,192,208,232,248,256,272,296,3..., dimensions={0} | all-to-all | bytes 786432 | tf_op jit(solution)/shard_map/all_to_all | solution.py:232
  94.1 0.2 convert_reduce_fusion.1
  94.3 0.2 fusion.6
  94.5 0.1 fusion.3
  94.6 0.1 broadcast_in_dim.17
  94.6 17.6 %all_to_all.33 = bf16[32,4,768]{2,1,0:T(4,128)(2,1)S(1)} all-to-all(bf16[32,4,768]{2,1,0:T(4,128)(2,1)S(1)} %broadcast_in_dim.17), channel_id=1, replica_groups={{0,16,40,56,64,80,104,120,128,144,168,184,192,208,232,248,256,272,296,3..., dimensions={0} | all-to-all | bytes 393216 | tf_op jit(solution)/shard_map/all_to_all | solution.py:232
  112.2 0.1 reshape.46.hidden
  112.2 0.3 narrow.1
  112.5 13.9 %all_to_all.34 = bf16[16,64,128]{2,1,0:T(8,128)(2,1)S(1)} all-to-all(bf16[16,64,128]{2,1,0:T(8,128)(2,1)S(1)} %bitcast.15), channel_id=1, replica_groups={{0,1,2,3,4,5,6,7,8,9,10,11,12,13,14,15},{16,17,18,19,20,21,22,23,24,25,..., dimensions={0} | all-to-all | bytes 524288 | tf_op jit(solution)/shard_map/all_to_all | solution.py:232
  126.5 0.6 fusion.1
  (2 shorter events, 0.1 us)
Async XLA Ops:
  0.6 56.1 %copy-start = (bf16[512,64]{0,1:T(8,128)(2,1)S(1)}, bf16[512,64]{0,1:T(8,128)(2,1)}, u32[]{:S(2)}) copy-start(bf16[512,64]{0,1:T(8,128)(2,1)} %param.25) | copy-start | bytes 196612
  2.6 34.5 %copy-start.1 = (f32[2,1,256,512]{3,2,1,0:T(8,128)S(1)}, f32[2,1,256,512]{3,2,1,0:T(8,128)}, u32[]{:S(2)}) copy-start(f32[2,1,256,512]{3,2,1,0:T(8,128)} %state.1) | copy-start | bytes 3145732
  37.8 34.4 %copy-start.2 = (f32[2,1,256,512]{3,2,1,0:T(8,128)}, f32[2,1,256,512]{3,2,1,0:T(8,128)S(1)}, u32[]{:S(2)}) copy-start(f32[2,1,256,512]{3,2,1,0:T(8,128)S(1)} %multiply_add_fusion._) | copy-start | bytes 3145732
  38.7 18.0 %all-to-all-start.1 = ((bf16[64,2,512]{2,1,0:T(2,128)(2,1)}), bf16[64,2,512]{2,1,0:T(2,128)(2,1)S(1)}, u32[]{:S(2)}, u32[]{:S(2)}) async-start(bf16[64,2,512]{2,1,0:T(2,128)(2,1)} %broadcast_in_dim.15), calls=%async_computation.1 | async-start | bytes 262144 | tf_op jit(solution)/shard_map/all_to_all | solution.py:232
  45.2 11.8 %collective-permute-start = (bf16[64,2560]{1,0:T(8,128)(2,1)S(1)}, bf16[64,2560]{1,0:T(8,128)(2,1)S(1)}, u32[]{:S(2)}, u32[]{:S(2)}) collective-permute-start(bf16[64,2560]{1,0:T(8,128)(2,1)S(1)} %get-tuple-element.25), channel_id=1, source_target_pairs={{0,8},{8,0},{16,24},{24,16},{32,40},{40,32},{48,56},{56,48},{64,72... | collective-permute-start | bytes 983048 | tf_op jit(solution)/shard_map/ppermute | solution.py:271

commit v4 on v3

--- a/solution.py
+++ b/solution.py
@@ -45,23 +45,26 @@
     return padded(units - cut_of(units) + 1)
 
 
-def project_kernel(*refs, count):
-    sources, outs = (refs[:count], refs[count : count + 5])
-    held, sems = (refs[count + 5 : -1] + outs[3:], refs[-1])
+def fetch(sources, held, sems):
     copies = [pltpu.make_async_copy(a, b, sems.at[i]) for i, (a, b) in enumerate(zip(sources, held))]
     for c in copies:
         c.start()
-    out_ref, mine_ref, sent_ref = outs[:3]
-    tok, gain, ffn_gain = held[:3]
-    weights, splits = (held[3:-5], held[-5:-2])
+    return copies
+
+
+def project_kernel(*refs, count, kept):
+    sources, out_ref = (refs[:count], refs[count])
+    held = refs[count + 1 + kept : -1] + refs[count + 1 : count + 1 + kept]
+    copies = fetch(sources, held, refs[-1])
+    tok, gain = held[:2]
     copies[0].wait()
     copies[1].wait()
     x = tok[...].astype(jnp.float32).T
     mix_in = (x * gain[...].astype(jnp.float32)).astype(jnp.bfloat16)
     squares = jnp.sum(x * x, axis=1, keepdims=True)
     at = 0
-    for i, w in enumerate(weights):
-        copies[3 + i].wait()
+    for copy, w in zip(copies[2 : count - kept], held[2 : count - kept]):
+        copy.wait()
         n = w.shape[1]
         part = jnp.dot(mix_in, w[...], preferred_element_type=jnp.float32)
         out_ref[:, at : at + n] = part.astype(jnp.bfloat16)
@@ -69,9 +72,34 @@
     rest = out_ref.shape[1] - at
     lane = lax.broadcasted_iota(jnp.int32, (x.shape[0], rest), 1)
     out_ref[:, at:] = jnp.where(lane == 0, squares, 0.0).astype(jnp.bfloat16)
-    copies[2].wait()
-    for c in copies[3 + len(weights) :]:
+    for copy in copies[count - kept :]:
+        copy.wait()
+
+
+def project(tok_t, gain, weights, kept):
+    total = sum(w.shape[1] for w in weights)
+    arrays = (tok_t, gain, *weights, *kept)
+    return pl.pallas_call(
+        functools.partial(project_kernel, count=len(arrays), kept=len(kept)),
+        out_shape=(
+            pltpu.VMEM((tok_t.shape[1], total + 128), jnp.bfloat16),
+            *(pltpu.VMEM(a.shape, a.dtype) for a in kept),
+        ),
+        in_specs=[pl.BlockSpec(memory_space=pl.ANY)] * len(arrays),
+        out_specs=whole(1 + len(kept)),
+        scratch_shapes=[pltpu.VMEM(a.shape, a.dtype) for a in arrays[: len(arrays) - len(kept)]]
+        + [pltpu.SemaphoreType.DMA((len(arrays),))],
+        name="project",
+    )(*arrays)
+
+
+def pack_kernel(_, *refs, count):
+    sources, outs = (refs[:count], refs[count : count + 2])
+    held, sems = (refs[count + 2 : -1], refs[-1])
+    for c in fetch(sources, held, sems):
         c.wait()
+    tok, ffn_gain, splits = (held[0], held[1], held[2:])
+    mine_ref, sent_ref = outs
     rows, units = splits[0].shape
     cut, half = (cut_of(units), half_of(units))
 
@@ -95,25 +123,20 @@
             fill(sent_ref, 1 - m, False)
 
 
-def project(tok_t, gain, ffn_gain, weights, splits, kept):
+def pack(after, tok_t, ffn_gain, splits):
     width, rows = tok_t.shape
-    total = sum(w.shape[1] for w in weights)
-    pack = len(splits) * half_of(splits[0].shape[1]) + rows + 2 * width
-    arrays = (tok_t, gain, ffn_gain, *weights, *splits, *kept)
-    return pl.pallas_call(
-        functools.partial(project_kernel, count=len(arrays)),
-        out_shape=(
-            pltpu.VMEM((rows, total + 128), jnp.bfloat16),
-            pltpu.VMEM((width, pack), jnp.bfloat16),
-            pltpu.VMEM((width, pack), jnp.bfloat16),
-            *(pltpu.VMEM(a.shape, a.dtype) for a in kept),
-        ),
-        in_specs=[pl.BlockSpec(memory_space=pl.ANY)] * len(arrays),
-        out_specs=whole(5),
-        scratch_shapes=[pltpu.VMEM(a.shape, a.dtype) for a in arrays[:-2]]
+    lanes = len(splits) * half_of(splits[0].shape[1]) + rows + 2 * width
+    arrays = (tok_t, ffn_gain, *splits)
+    return pl.pallas_call(
+        functools.partial(pack_kernel, count=len(arrays)),
+        out_shape=(pltpu.VMEM((width, lanes), jnp.bfloat16),) * 2,
+        in_specs=whole(1) + [pl.BlockSpec(memory_space=pl.ANY)] * len(arrays),
+        out_specs=whole(2),
+        scratch_shapes=[pltpu.VMEM(a.shape, a.dtype) for a in arrays]
         + [pltpu.SemaphoreType.DMA((len(arrays),))],
-        name="project",
-    )(*arrays)
+        compiler_params=pltpu.CompilerParams(vmem_limit_bytes=8 << 20),
+        name="pack",
+    )(in_vmem(after), *arrays)
 
 
 def attend_kernel(sums, bias, gain, state, key_ref, value_ref, decay_ref, out_ref, *, model_width):
@@ -159,6 +182,7 @@
         ),
         in_specs=whole(4),
         out_specs=whole(4),
+        compiler_params=pltpu.CompilerParams(vmem_limit_bytes=8 << 20),
         name="attend",
     )(*(in_vmem(a) for a in (sums, bias, gain, state)))
 
@@ -198,6 +222,7 @@
         ),
         in_specs=whole(4),
         out_specs=whole(2),
+        compiler_params=pltpu.CompilerParams(vmem_limit_bytes=8 << 20),
         name="widen",
     )(*(in_vmem(a) for a in (parts, mine, got, new_state)))
 
@@ -224,6 +249,7 @@
         out_shape=pltpu.VMEM((2, tp, width, seqs), jnp.bfloat16),
         in_specs=whole(3),
         out_specs=pl.BlockSpec(memory_space=pltpu.VMEM),
+        compiler_params=pltpu.CompilerParams(vmem_limit_bytes=8 << 20),
         name="narrow",
     )(*(in_vmem(a) for a in (hidden, mine, got)))
 
@@ -260,26 +286,25 @@
     own_rows, heads, _, val_dim = state.shape
     kv, tp = (lax.axis_size(a) for a in ("kv", "tp"))
     model_width = tokens.shape[1] * kv
-    made, mine, sent, bias, head_scale = project(
+    made, bias, head_scale = project(
         tokens.T,
         mix_gain[None, :],
-        ffn_gain[None, :],
         (w_query, w_key, w_value, w_gate, w_decay),
-        (w_ffgate, w_ffup, w_down.T),
         (decay_bias[None, :], head_gain.reshape(-1, 128)),
     )
-    got = lax.ppermute(sent, "kv", [(i, i ^ 1) for i in range(kv)])
     arrived = exchanged(made.reshape(kv, own_rows, -1), "kv")
     keys, values, decay, head_out = attend(summed(arrived), bias, head_scale, state, model_width)
+    heads_all = exchanged(copies_of(head_out, kv), "kv")
+    mine, sent = pack(head_out, tokens.T, ffn_gain[None, :], (w_ffgate, w_ffup, w_down.T))
+    got = lax.ppermute(sent, "kv", [(i, i ^ 1) for i in range(kv)])
     new_state = (
         decay[:, None, :, None] * state + keys[:, None, :, None] * values[:, None, None, :]
     )
-    head_out, new_state = lax.optimization_barrier((head_out, new_state))
-    heads_all = exchanged(copies_of(head_out, kv), "kv").reshape(-1, heads * val_dim)
+    heads_all = heads_all.reshape(-1, heads * val_dim)
     attn_part = lax.dot_general(
         w_output, heads_all, (((0,), (1,)), ((), ())), preferred_element_type=jnp.float32
     ).astype(jnp.bfloat16)
-    attn_part, got = lax.optimization_barrier((attn_part, got))
+    attn_part, got, new_state = lax.optimization_barrier((attn_part, got, new_state))
     width, seqs = attn_part.shape
     pair, line = (pairs(kv, tp), lines(kv))
     attn_parts = exchanged(copies_of(attn_part, 2 * tp), ("kv", "tp"), pair)

time: 127 us -> 128 us (level)
  waiting for transfers between devices: 8.63 us -> 6.86 us
    all_to_all x1, waiting for transfers between devices: 8.62 us -> 6.86 us  [exchanged(): lax.all_to_all(blocks, axis, 0, 0, axis_index_groups=groups, tiled=True)]
    pallas_call x1 -> x2, Pallas kernels: 1.96 us -> 2.67 us  [the longest x1 1.8 us: project(): pl.pallas_call(functools.partial(project_kernel, count=len(arrays), kept=...]
  transfers between devices with their start and end apart: 2 -> 2, of which waited for: 1 -> 1; matrix products, arithmetic and copies ran while one was open for 0% -> 0% of each run, Pallas kernels for 0% -> 1%
where the time goes in v4:
time: 128 us
  blocking collectives  103 us (80%)
  starting transfers between devices  9.54 us (7%)
  waiting for transfers between devices  6.86 us (5%)
  Pallas kernels  3.74 us (3%)
  local copies, waits for them, and re-layouts  1.85 us (1%)
  other arithmetic  1.73 us (1%)
    all_to_all x5, blocking collectives, exchanged(): lax.all_to_all(blocks, axis, 0, 0, axis_index_groups=groups, tiled=True)  103 us
    all_to_all x1, waiting for transfers between devices, exchanged(): lax.all_to_all(blocks, axis, 0, 0, axis_index_groups=groups, tiled=True)  6.86 us
    all_to_all x1, starting transfers between devices, exchanged(): lax.all_to_all(blocks, axis, 0, 0, axis_index_groups=groups, tiled=True)  6.62 us
    ppermute x1, starting transfers between devices, local(): got = lax.ppermute(sent, 'kv', [(i, i ^ 1) for i in range(kv)])  2.93 us
  transfers between devices with their start and end apart: 2, of which 1 were waited for; matrix products, arithmetic and copies ran while one was open for 0% of the time, Pallas kernels for 1%

profile of v4, /device:TPU:1, one launch (start us, length us, event | category | flops | bytes accessed | tf_op | source)
XLA Modules:
  0.0 127.8 jit_solution(11799403043834555812)
XLA Ops:
  0.6 0.0 copy-start
  0.6 1.8 %project.1 = (bf16[128,1920]{1,0:T(8,128)(2,1)S(1)}, f32[1,256]{1,0:T(1,128)S(1)}, bf16[4,128]{1,0:T(4,128)(2,1)S(1)}) custom-call(bf16[64,128]{1,0:T(8,128)(2,1)} %bitcast.17, bf16[1,64]{1,0:T(2,128)(2,1)} %bitcast.22, bf16[64,256]{1,0:T(8,128)(2,1)} %refs_2_.2, bf16[64,256]{1,0:T(8,128)(2,1)} %refs_3_.2, bf16[64,512]{1,0:T(8,128)(2,1)} %refs_4_.1, ...), custom_call_target="tpu_custom_call" | custom-call | tf_op jit(solution)/shard_map/project/pallas_call | solution.py:82
  2.5 0.0 copy-start.1
  2.5 0.2 reshape.42
  2.7 33.8 %all_to_all.30 = bf16[64,2,1920]{2,1,0:T(2,128)(2,1)S(1)} all-to-all(bf16[64,2,1920]{2,1,0:T(2,128)(2,1)S(1)} %reshape.42), channel_id=1, replica_groups=mesh['kv'=64,'tp'=8] {'kv'}, dimensions={0} | all-to-all | bytes 983040 | tf_op jit(solution)/shard_map/all_to_all | solution.py:258
  36.5 0.4 convert_reduce_fusion.sums
  36.9 0.0 copy-done.1
  36.9 0.0 copy-start.5
  36.9 0.5 attend.1
  37.4 0.0 copy-start.3
  37.4 0.0 copy-start.4
  37.4 0.7 broadcast_in_dim.14
  38.1 0.0 copy-start.6
  38.1 6.6 %all-to-all-start.1 = ((bf16[64,2,512]{2,1,0:T(2,128)(2,1)}), bf16[64,2,512]{2,1,0:T(2,128)(2,1)S(1)}, u32[]{:S(2)}, u32[]{:S(2)}) async-start(bf16[64,2,512]{2,1,0:T(2,128)(2,1)} %broadcast_in_dim.14), calls=%async_computation.1 | async-start | bytes 262144 | tf_op jit(solution)/shard_map/all_to_all | solution.py:258
  44.8 0.0 copy-start.7
  44.8 0.0 copy-done.5
  44.8 0.0 copy-done.3
  44.8 0.0 copy-done.4
  44.8 0.0 copy-done.6
  44.8 0.6 copy-done.7
  45.4 0.9 pack.1
  46.3 2.9 %collective-permute-start = (bf16[64,2560]{1,0:T(8,128)(2,1)S(1)}, bf16[64,2560]{1,0:T(8,128)(2,1)S(1)}, u32[]{:S(2)}, u32[]{:S(2)}) collective-permute-start(bf16[64,2560]{1,0:T(8,128)(2,1)S(1)} %get-tuple-element.20), channel_id=1, source_target_pairs={{0,8},{8,0},{16,24},{24,16},{32,40},{40,32},{48,56},{56,48},{64,72... | collective-permute-start | bytes 983048 | tf_op jit(solution)/shard_map/ppermute | solution.py:299
  49.2 0.2 multiply_add_fusion._
  49.4 0.0 copy-start.2
  49.5 6.9 %all-to-all-done.1 = bf16[64,2,512]{2,1,0:T(2,128)(2,1)S(1)} async-done(((bf16[64,2,512]{2,1,0:T(2,128)(2,1)}), bf16[64,2,512]{2,1,0:T(2,128)(2,1)S(1)}, u32[]{:S(2)}, u32[]{:S(2)}) %all-to-all-start.1) | async-done | bytes 131104 | tf_op jit(solution)/shard_map/all_to_all | solution.py:258
  56.3 0.1 reshape.43
  56.4 0.0 copy-done
  56.4 0.2 fusion
  56.5 0.0 collective-permute-done.got
  56.6 14.4 %all_to_all.31 = bf16[16,64,128]{2,1,0:T(8,128)(2,1)S(1)} all-to-all(bf16[16,64,128]{2,1,0:T(8,128)(2,1)S(1)} %broadcast_in_dim.16), channel_id=1, replica_groups={{0,1,2,3,4,5,6,7,8,9,10,11,12,13,14,15},{16,17,18,19,20,21,22,23,24,25,..., dimensions={0} | all-to-all | bytes 524288 | tf_op jit(solution)/shard_map/all_to_all | solution.py:258
  71.0 0.3 widen.1
  71.3 0.0 copy-done.2
  71.3 0.1 reshape.45
  71.4 23.3 %all_to_all.32 = bf16[32,4,1536]{2,1,0:T(4,128)(2,1)S(1)} all-to-all(bf16[32,4,1536]{2,1,0:T(4,128)(2,1)S(1)} %reshape.45), channel_id=1, replica_groups={{0,16,40,56,64,80,104,120,128,144,168,184,192,208,232,248,256,272,296,3..., dimensions={0} | all-to-all | bytes 786432 | tf_op jit(solution)/shard_map/all_to_all | solution.py:258
  94.8 0.2 convert_reduce_fusion.1
  94.9 0.2 fusion.6
  95.1 0.1 fusion.3
  95.2 0.1 broadcast_in_dim.17
  95.3 17.7 %all_to_all.33 = bf16[32,4,768]{2,1,0:T(4,128)(2,1)S(1)} all-to-all(bf16[32,4,768]{2,1,0:T(4,128)(2,1)S(1)} %broadcast_in_dim.17), channel_id=1, replica_groups={{0,16,40,56,64,80,104,120,128,144,168,184,192,208,232,248,256,272,296,3..., dimensions={0} | all-to-all | bytes 393216 | tf_op jit(solution)/shard_map/all_to_all | solution.py:258
  112.9 0.1 reshape.46.hidden
  113.0 0.3 narrow.1
  113.3 13.9 %all_to_all.34 = bf16[16,64,128]{2,1,0:T(8,128)(2,1)S(1)} all-to-all(bf16[16,64,128]{2,1,0:T(8,128)(2,1)S(1)} %bitcast.15), channel_id=1, replica_groups={{0,1,2,3,4,5,6,7,8,9,10,11,12,13,14,15},{16,17,18,19,20,21,22,23,24,25,..., dimensions={0} | all-to-all | bytes 524288 | tf_op jit(solution)/shard_map/all_to_all | solution.py:258
  127.2 0.6 fusion.1
  (2 shorter events, 0.1 us)
Async XLA Ops:
  0.6 55.7 %copy-start = (bf16[512,64]{0,1:T(8,128)(2,1)S(1)}, bf16[512,64]{0,1:T(8,128)(2,1)}, u32[]{:S(2)}) copy-start(bf16[512,64]{0,1:T(8,128)(2,1)} %param.25) | copy-start | bytes 196612
  2.5 34.4 %copy-start.1 = (f32[2,1,256,512]{3,2,1,0:T(8,128)S(1)}, f32[2,1,256,512]{3,2,1,0:T(8,128)}, u32[]{:S(2)}) copy-start(f32[2,1,256,512]{3,2,1,0:T(8,128)} %state.1) | copy-start | bytes 3145732
  36.9 7.9 %copy-start.5 = (bf16[1376,64]{0,1:T(8,128)(2,1)S(1)}, bf16[1376,64]{0,1:T(8,128)(2,1)}, u32[]{:S(2)}) copy-start(bf16[1376,64]{0,1:T(8,128)(2,1)} %param.28) | copy-start | bytes 528388
  37.4 7.4 %copy-start.3 = (bf16[64,1376]{1,0:T(8,128)(2,1)S(1)}, bf16[64,1376]{1,0:T(8,128)(2,1)}, u32[]{:S(2)}) copy-start(bf16[64,1376]{1,0:T(8,128)(2,1)} %refs_2_.3) | copy-start | bytes 528388
  37.4 7.4 %copy-start.4 = (bf16[64,1376]{1,0:T(8,128)(2,1)S(1)}, bf16[64,1376]{1,0:T(8,128)(2,1)}, u32[]{:S(2)}) copy-start(bf16[64,1376]{1,0:T(8,128)(2,1)} %refs_3_.3) | copy-start | bytes 528388
  38.1 6.7 %copy-start.6 = (bf16[128,64]{0,1:T(8,128)(2,1)S(1)}, bf16[128,64]{0,1:T(8,128)(2,1)}, u32[]{:S(2)}) copy-start(bf16[128,64]{0,1:T(8,128)(2,1)} %param.15) | copy-start | bytes 49156
  38.1 18.2 %all-to-all-start.1 = ((bf16[64,2,512]{2,1,0:T(2,128)(2,1)}), bf16[64,2,512]{2,1,0:T(2,128)(2,1)S(1)}, u32[]{:S(2)}, u32[]{:S(2)}) async-start(bf16[64,2,512]{2,1,0:T(2,128)(2,1)} %broadcast_in_dim.14), calls=%async_computation.1 | async-start | bytes 262144 | tf_op jit(solution)/shard_map/all_to_all | solution.py:258
  44.8 0.7 copy-start.7
  46.3 10.3 %collective-permute-start = (bf16[64,2560]{1,0:T(8,128)(2,1)S(1)}, bf16[64,2560]{1,0:T(8,128)(2,1)S(1)}, u32[]{:S(2)}, u32[]{:S(2)}) collective-permute-start(bf16[64,2560]{1,0:T(8,128)(2,1)S(1)} %get-tuple-element.20), channel_id=1, source_target_pairs={{0,8},{8,0},{16,24},{24,16},{32,40},{40,32},{48,56},{56,48},{64,72... | collective-permute-start | bytes 983048 | tf_op jit(solution)/shard_map/ppermute | solution.py:299
  49.4 21.9 %copy-start.2 = (f32[2,1,256,512]{3,2,1,0:T(8,128)}, f32[2,1,256,512]{3,2,1,0:T(8,128)S(1)}, u32[]{:S(2)}) copy-start(f32[2,1,256,512]{3,2,1,0:T(8,128)S(1)} %multiply_add_fusion._) | copy-start | bytes 3145732

commit v5 on v4

--- a/solution.py
+++ b/solution.py
@@ -93,13 +93,8 @@
     )(*arrays)
 
 
-def pack_kernel(_, *refs, count):
-    sources, outs = (refs[:count], refs[count : count + 2])
-    held, sems = (refs[count + 2 : -1], refs[-1])
-    for c in fetch(sources, held, sems):
-        c.wait()
-    tok, ffn_gain, splits = (held[0], held[1], held[2:])
-    mine_ref, sent_ref = outs
+def pack_kernel(_, tok, ffn_gain, *refs):
+    splits, (mine_ref, sent_ref) = (refs[:-2], refs[-2:])
     rows, units = splits[0].shape
     cut, half = (cut_of(units), half_of(units))
 
@@ -126,17 +121,15 @@
 def pack(after, tok_t, ffn_gain, splits):
     width, rows = tok_t.shape
     lanes = len(splits) * half_of(splits[0].shape[1]) + rows + 2 * width
-    arrays = (tok_t, ffn_gain, *splits)
-    return pl.pallas_call(
-        functools.partial(pack_kernel, count=len(arrays)),
+    arrays = (after, tok_t, ffn_gain, *splits)
+    return pl.pallas_call(
+        pack_kernel,
         out_shape=(pltpu.VMEM((width, lanes), jnp.bfloat16),) * 2,
-        in_specs=whole(1) + [pl.BlockSpec(memory_space=pl.ANY)] * len(arrays),
+        in_specs=whole(len(arrays)),
         out_specs=whole(2),
-        scratch_shapes=[pltpu.VMEM(a.shape, a.dtype) for a in arrays]
-        + [pltpu.SemaphoreType.DMA((len(arrays),))],
         compiler_params=pltpu.CompilerParams(vmem_limit_bytes=8 << 20),
         name="pack",
-    )(in_vmem(after), *arrays)
+    )(*(in_vmem(a) for a in arrays))
 
 
 def attend_kernel(sums, bias, gain, state, key_ref, value_ref, decay_ref, out_ref, *, model_width):
@@ -187,6 +180,21 @@
     )(*(in_vmem(a) for a in (sums, bias, gain, state)))
 
 
+def total_kernel(parts, out_ref):
+    out_ref[...] = jnp.sum(parts[...].astype(jnp.float32), axis=1)
+
+
+def total(parts):
+    return pl.pallas_call(
+        total_kernel,
+        out_shape=pltpu.VMEM((parts.shape[0], *parts.shape[2:]), jnp.float32),
+        in_specs=whole(1),
+        out_specs=pl.BlockSpec(memory_space=pltpu.VMEM),
+        compiler_params=pltpu.CompilerParams(vmem_limit_bytes=8 << 20),
+        name="total",
+    )(in_vmem(parts))
+
+
 def widen_kernel(parts, mine, got, _, out_ref, mid_ref):
     r = member(lax.axis_index("kv"))
     _, seqs = mid_ref.shape
@@ -194,8 +202,7 @@
     end = 3 * half
 
     def mid_of(ref, at):
-        total = jnp.sum(parts[at].astype(jnp.float32), axis=0)
-        return (ref[:, end : end + seqs].astype(jnp.float32) + total).astype(jnp.bfloat16)
+        return (ref[:, end : end + seqs].astype(jnp.float32) + parts[at]).astype(jnp.bfloat16)
 
     own = mid_of(mine, r)
     mid_ref[...] = own
@@ -213,7 +220,7 @@
 
 
 def widen(parts, mine, got, new_state, half):
-    width, seqs = parts.shape[2:]
+    width, seqs = parts.shape[1:]
     return pl.pallas_call(
         widen_kernel,
         out_shape=(
@@ -286,16 +293,16 @@
     own_rows, heads, _, val_dim = state.shape
     kv, tp = (lax.axis_size(a) for a in ("kv", "tp"))
     model_width = tokens.shape[1] * kv
-    made, bias, head_scale = project(
+    made, bias, head_scale, ffn_scale = project(
         tokens.T,
         mix_gain[None, :],
         (w_query, w_key, w_value, w_gate, w_decay),
-        (decay_bias[None, :], head_gain.reshape(-1, 128)),
+        (decay_bias[None, :], head_gain.reshape(-1, 128), ffn_gain[None, :]),
     )
     arrived = exchanged(made.reshape(kv, own_rows, -1), "kv")
     keys, values, decay, head_out = attend(summed(arrived), bias, head_scale, state, model_width)
     heads_all = exchanged(copies_of(head_out, kv), "kv")
-    mine, sent = pack(head_out, tokens.T, ffn_gain[None, :], (w_ffgate, w_ffup, w_down.T))
+    mine, sent = pack(head_out, tokens.T, ffn_scale, (w_ffgate, w_ffup, w_down.T))
     got = lax.ppermute(sent, "kv", [(i, i ^ 1) for i in range(kv)])
     new_state = (
         decay[:, None, :, None] * state + keys[:, None, :, None] * values[:, None, None, :]
@@ -304,12 +311,13 @@
     attn_part = lax.dot_general(
         w_output, heads_all, (((0,), (1,)), ((), ())), preferred_element_type=jnp.float32
     ).astype(jnp.bfloat16)
-    attn_part, got, new_state = lax.optimization_barrier((attn_part, got, new_state))
+    attn_part, new_state = lax.optimization_barrier((attn_part, new_state))
     width, seqs = attn_part.shape
     pair, line = (pairs(kv, tp), lines(kv))
     attn_parts = exchanged(copies_of(attn_part, 2 * tp), ("kv", "tp"), pair)
     half = half_of(w_ffgate.shape[1])
-    wide, mid_t = widen(attn_parts.reshape(2, tp, width, seqs), mine, got, new_state, half)
+    attn_sums = total(attn_parts.reshape(2, tp, width, seqs))
+    wide, mid_t = widen(attn_sums, mine, got, new_state, half)
     count = len(line[0])
     sums = summed(exchanged(wide.reshape(count, seqs // count, -1), "kv", line))
     ffn_rms = lax.rsqrt(sums[:, half - 1 : half] / model_width + epsilon)

time: 128 us -> 128 us (level)
  blocking collectives: 103 us -> 82.5 us
  waiting for transfers between devices: 6.86 us -> 19.9 us
  starting transfers between devices: 9.54 us -> 17.3 us
    all_to_all x5 -> x4, blocking collectives: 103 us -> 82.5 us  [exchanged(): lax.all_to_all(blocks, axis, 0, 0, axis_index_groups=groups, tiled=True)]
    all_to_all x1 -> x2, waiting for transfers between devices: 6.86 us -> 15.1 us  [exchanged(): lax.all_to_all(blocks, axis, 0, 0, axis_index_groups=groups, tiled=True)]
    all_to_all x1 -> x2, starting transfers between devices: 6.62 us -> 14 us  [exchanged(): lax.all_to_all(blocks, axis, 0, 0, axis_index_groups=groups, tiled=True)]
    ppermute x1, waiting for transfers between devices: 0.01 us -> 4.78 us  [local(): got = lax.ppermute(sent, 'kv', [(i, i ^ 1) for i in range(kv)])]
  transfers between devices with their start and end apart: 2 -> 3, of which waited for: 1 -> 3; matrix products, arithmetic and copies ran while one was open for 0% -> 0% of each run, Pallas kernels for 1% -> 0%
where the time goes in v5:
time: 128 us; the launch traced here: 127 us
  blocking collectives  82.5 us (64%)
  waiting for transfers between devices  19.9 us (16%)
  starting transfers between devices  17.3 us (14%)
  Pallas kernels  3.04 us (2%)
  local copies, waits for them, and re-layouts  1.97 us (2%)
  other arithmetic  1.73 us (1%)
    all_to_all x4, blocking collectives, exchanged(): lax.all_to_all(blocks, axis, 0, 0, axis_index_groups=groups, tiled=True)  82.5 us
    all_to_all x2, waiting for transfers between devices, exchanged(): lax.all_to_all(blocks, axis, 0, 0, axis_index_groups=groups, tiled=True)  15.1 us
    all_to_all x2, starting transfers between devices, exchanged(): lax.all_to_all(blocks, axis, 0, 0, axis_index_groups=groups, tiled=True)  14 us
    ppermute x1, waiting for transfers between devices, local(): got = lax.ppermute(sent, 'kv', [(i, i ^ 1) for i in range(kv)])  4.78 us
    ppermute x1, starting transfers between devices, local(): got = lax.ppermute(sent, 'kv', [(i, i ^ 1) for i in range(kv)])  3.26 us
  transfers between devices with their start and end apart: 3, of which 3 were waited for; matrix products, arithmetic and copies ran while one was open for 0% of the time, Pallas kernels for 0%

profile of v5, /device:TPU:1, one launch (start us, length us, event | category | flops | bytes accessed | tf_op | source)
XLA Modules:
  0.0 127.4 jit_solution(9160501119998804919)
XLA Ops:
  0.6 0.0 copy-start
  0.6 1.8 %project.1 = (bf16[128,1920]{1,0:T(8,128)(2,1)S(1)}, f32[1,256]{1,0:T(1,128)S(1)}, bf16[4,128]{1,0:T(4,128)(2,1)S(1)}, bf16[1,64]{1,0:T(2,128)(2,1)S(1)}) custom-call(bf16[64,128]{1,0:T(8,128)(2,1)} %bitcast.17, bf16[1,64]{1,0:T(2,128)(2,1)} %bitcast.21, bf16[64,256]{1,0:T(8,128)(2,1)} %refs_2_.1, bf16[64,256]{1,0:T(8,128)(2,1)} %refs_3_.1, ...), custom_call_target="tpu_custom_call" | custom-call | tf_op jit(solution)/shard_map/project/pallas_call | solution.py:82
  2.5 0.0 copy-start.2
  2.5 0.2 reshape.42
  2.7 33.8 %all_to_all.30 = bf16[64,2,1920]{2,1,0:T(2,128)(2,1)S(1)} all-to-all(bf16[64,2,1920]{2,1,0:T(2,128)(2,1)S(1)} %reshape.42), channel_id=1, replica_groups=mesh['kv'=64,'tp'=8] {'kv'}, dimensions={0} | all-to-all | bytes 983040 | tf_op jit(solution)/shard_map/all_to_all | solution.py:265
  36.5 0.4 convert_reduce_fusion.sums
  36.9 0.0 copy-done.2
  36.9 0.5 attend.1
  37.4 0.7 broadcast_in_dim.15
  38.1 6.5 %all-to-all-start.1 = ((bf16[64,2,512]{2,1,0:T(2,128)(2,1)}), bf16[64,2,512]{2,1,0:T(2,128)(2,1)S(1)}, u32[]{:S(2)}, u32[]{:S(2)}) async-start(bf16[64,2,512]{2,1,0:T(2,128)(2,1)} %broadcast_in_dim.15), calls=%async_computation.1 | async-start | bytes 262144 | tf_op jit(solution)/shard_map/all_to_all | solution.py:265
  44.6 0.2 multiply_add_fusion._
  44.8 0.0 copy-start.1
  44.9 11.3 %all-to-all-done.1 = bf16[64,2,512]{2,1,0:T(2,128)(2,1)S(1)} async-done(((bf16[64,2,512]{2,1,0:T(2,128)(2,1)}), bf16[64,2,512]{2,1,0:T(2,128)(2,1)S(1)}, u32[]{:S(2)}, u32[]{:S(2)}) %all-to-all-start.1) | async-done | bytes 131104 | tf_op jit(solution)/shard_map/all_to_all | solution.py:265
  56.2 0.1 reshape.43
  56.2 0.0 copy-done
  56.3 0.2 fusion
  56.4 0.0 copy-start.5
  56.4 0.7 broadcast_in_dim.16
  57.2 0.0 copy-start.3
  57.2 0.0 copy-start.4
  57.2 0.0 copy-start.6
  57.2 7.5 %all-to-all-start.2 = ((bf16[16,64,128]{2,1,0:T(8,128)(2,1)}), bf16[16,64,128]{2,1,0:T(8,128)(2,1)S(1)}, u32[]{:S(2)}, u32[]{:S(2)}) async-start(bf16[16,64,128]{2,1,0:T(8,128)(2,1)} %broadcast_in_dim.16), calls=%async_computation.2 | async-start | bytes 524288 | tf_op jit(solution)/shard_map/all_to_all | solution.py:265
  64.7 0.0 copy-done.5
  64.7 0.0 copy-done.3
  64.7 0.0 copy-done.4
  64.7 0.0 copy-done.6
  64.8 0.1 pack.1
  64.9 3.3 %collective-permute-start = (bf16[64,2560]{1,0:T(8,128)(2,1)S(1)}, bf16[64,2560]{1,0:T(8,128)(2,1)S(1)}, u32[]{:S(2)}, u32[]{:S(2)}) collective-permute-start(bf16[64,2560]{1,0:T(8,128)(2,1)S(1)} %get-tuple-element.26), channel_id=1, source_target_pairs={{0,8},{8,0},{16,24},{24,16},{32,40},{40,32},{48,56},{56,48},{64,72... | collective-permute-start | bytes 983048 | tf_op jit(solution)/shard_map/ppermute | solution.py:306
  68.1 3.8 %all-to-all-done.2 = bf16[16,64,128]{2,1,0:T(8,128)(2,1)S(1)} async-done(((bf16[16,64,128]{2,1,0:T(8,128)(2,1)}), bf16[16,64,128]{2,1,0:T(8,128)(2,1)S(1)}, u32[]{:S(2)}, u32[]{:S(2)}) %all-to-all-start.2) | async-done | bytes 262176 | tf_op jit(solution)/shard_map/all_to_all | solution.py:265
  72.0 4.8 %collective-permute-done.got = bf16[64,2560]{1,0:T(8,128)(2,1)S(1)} collective-permute-done((bf16[64,2560]{1,0:T(8,128)(2,1)S(1)}, bf16[64,2560]{1,0:T(8,128)(2,1)S(1)}, u32[]{:S(2)}, u32[]{:S(2)}) %collective-permute-start) | collective-permute-done | bytes 327712 | tf_op jit(solution)/shard_map/ppermute | solution.py:306
  76.8 0.0 copy-done.1
  76.8 0.3 widen.1
  77.1 0.1 reshape.45
  77.2 17.8 %all_to_all.31 = bf16[32,4,1536]{2,1,0:T(4,128)(2,1)S(1)} all-to-all(bf16[32,4,1536]{2,1,0:T(4,128)(2,1)S(1)} %reshape.45), channel_id=1, replica_groups={{0,16,40,56,64,80,104,120,128,144,168,184,192,208,232,248,256,272,296,3..., dimensions={0} | all-to-all | bytes 786432 | tf_op jit(solution)/shard_map/all_to_all | solution.py:265
  95.0 0.2 convert_reduce_fusion.1
  95.2 0.2 fusion.6
  95.4 0.1 fusion.3
  95.5 0.1 broadcast_in_dim.17
  95.5 15.8 %all_to_all.32 = bf16[32,4,768]{2,1,0:T(4,128)(2,1)S(1)} all-to-all(bf16[32,4,768]{2,1,0:T(4,128)(2,1)S(1)} %broadcast_in_dim.17), channel_id=1, replica_groups={{0,16,40,56,64,80,104,120,128,144,168,184,192,208,232,248,256,272,296,3..., dimensions={0} | all-to-all | bytes 393216 | tf_op jit(solution)/shard_map/all_to_all | solution.py:265
  111.3 0.1 reshape.46.hidden
  111.3 0.3 narrow.1
  111.6 15.2 %all_to_all.33 = bf16[16,64,128]{2,1,0:T(8,128)(2,1)S(1)} all-to-all(bf16[16,64,128]{2,1,0:T(8,128)(2,1)S(1)} %bitcast.14), channel_id=1, replica_groups={{0,1,2,3,4,5,6,7,8,9,10,11,12,13,14,15},{16,17,18,19,20,21,22,23,24,25,..., dimensions={0} | all-to-all | bytes 524288 | tf_op jit(solution)/shard_map/all_to_all | solution.py:265
  126.8 0.6 fusion.1
  (2 shorter events, 0.1 us)
Async XLA Ops:
  0.6 55.6 %copy-start = (bf16[512,64]{0,1:T(8,128)(2,1)S(1)}, bf16[512,64]{0,1:T(8,128)(2,1)}, u32[]{:S(2)}) copy-start(bf16[512,64]{0,1:T(8,128)(2,1)} %param.25) | copy-start | bytes 196612
  2.5 34.4 %copy-start.2 = (f32[2,1,256,512]{3,2,1,0:T(8,128)S(1)}, f32[2,1,256,512]{3,2,1,0:T(8,128)}, u32[]{:S(2)}) copy-start(f32[2,1,256,512]{3,2,1,0:T(8,128)} %state.1) | copy-start | bytes 3145732
  38.1 18.0 %all-to-all-start.1 = ((bf16[64,2,512]{2,1,0:T(2,128)(2,1)}), bf16[64,2,512]{2,1,0:T(2,128)(2,1)S(1)}, u32[]{:S(2)}, u32[]{:S(2)}) async-start(bf16[64,2,512]{2,1,0:T(2,128)(2,1)} %broadcast_in_dim.15), calls=%async_computation.1 | async-start | bytes 262144 | tf_op jit(solution)/shard_map/all_to_all | solution.py:265
  44.8 31.9 %copy-start.1 = (f32[2,1,256,512]{3,2,1,0:T(8,128)}, f32[2,1,256,512]{3,2,1,0:T(8,128)S(1)}, u32[]{:S(2)}) copy-start(f32[2,1,256,512]{3,2,1,0:T(8,128)S(1)} %multiply_add_fusion._) | copy-start | bytes 3145732
  56.4 8.3 %copy-start.5 = (bf16[1376,64]{0,1:T(8,128)(2,1)S(1)}, bf16[1376,64]{0,1:T(8,128)(2,1)}, u32[]{:S(2)}) copy-start(bf16[1376,64]{0,1:T(8,128)(2,1)} %param.28) | copy-start | bytes 528388
  57.2 7.5 %copy-start.3 = (bf16[64,1376]{1,0:T(8,128)(2,1)S(1)}, bf16[64,1376]{1,0:T(8,128)(2,1)}, u32[]{:S(2)}) copy-start(bf16[64,1376]{1,0:T(8,128)(2,1)} %refs_0_.1) | copy-start | bytes 528388
  57.2 7.6 %copy-start.4 = (bf16[64,1376]{1,0:T(8,128)(2,1)S(1)}, bf16[64,1376]{1,0:T(8,128)(2,1)}, u32[]{:S(2)}) copy-start(bf16[64,1376]{1,0:T(8,128)(2,1)} %refs_1_.1) | copy-start | bytes 528388
  57.2 7.6 %copy-start.6 = (bf16[128,64]{0,1:T(8,128)(2,1)S(1)}, bf16[128,64]{0,1:T(8,128)(2,1)}, u32[]{:S(2)}) copy-start(bf16[128,64]{0,1:T(8,128)(2,1)} %param.15) | copy-start | bytes 49156
  57.2 14.8 %all-to-all-start.2 = ((bf16[16,64,128]{2,1,0:T(8,128)(2,1)}), bf16[16,64,128]{2,1,0:T(8,128)(2,1)S(1)}, u32[]{:S(2)}, u32[]{:S(2)}) async-start(bf16[16,64,128]{2,1,0:T(8,128)(2,1)} %broadcast_in_dim.16), calls=%async_computation.2 | async-start | bytes 524288 | tf_op jit(solution)/shard_map/all_to_all | solution.py:265
  64.9 11.9 %collective-permute-start = (bf16[64,2560]{1,0:T(8,128)(2,1)S(1)}, bf16[64,2560]{1,0:T(8,128)(2,1)S(1)}, u32[]{:S(2)}, u32[]{:S(2)}) collective-permute-start(bf16[64,2560]{1,0:T(8,128)(2,1)S(1)} %get-tuple-element.26), channel_id=1, source_target_pairs={{0,8},{8,0},{16,24},{24,16},{32,40},{40,32},{48,56},{56,48},{64,72... | collective-permute-start | bytes 983048 | tf_op jit(solution)/shard_map/ppermute | solution.py:306

commit v6 on v5

--- a/solution.py
+++ b/solution.py
@@ -37,12 +37,9 @@
     return [pl.BlockSpec(memory_space=pltpu.VMEM)] * count
 
 
-def cut_of(units):
-    return units // 256 * 128
-
-
-def half_of(units):
-    return padded(units - cut_of(units) + 1)
+def widths(units):
+    half = units // 2
+    return half, padded(2 * half + 1), padded(half)
 
 
 def fetch(sources, held, sems):
@@ -96,15 +93,17 @@
 def pack_kernel(_, tok, ffn_gain, *refs):
     splits, (mine_ref, sent_ref) = (refs[:-2], refs[-2:])
     rows, units = splits[0].shape
-    cut, half = (cut_of(units), half_of(units))
+    seqs = tok.shape[1]
+    half, both, alone = widths(units)
 
     def fill(ref, m, first):
-        a, b = ((0, cut), (cut, units))[m]
-        for i, w in enumerate(splits):
-            ref[:, i * half : i * half + b - a] = w[:, a:b]
-            ref[:, i * half + b - a : (i + 1) * half] = jnp.zeros((rows, half - (b - a)), w.dtype)
-        seqs = tok.shape[1]
-        end = len(splits) * half
+        gate, up, down = (w[:, m * half : (m + 1) * half] for w in splits)
+        ref[:, :half] = gate
+        ref[:, half : 2 * half] = up
+        ref[:, 2 * half : both] = jnp.zeros((rows, both - 2 * half), ref.dtype)
+        ref[:, both : both + half] = down
+        ref[:, both + half : both + alone] = jnp.zeros((rows, alone - half), ref.dtype)
+        end = both + alone
         ref[:, end : end + seqs] = tok[...]
         ref[:, end + seqs :] = jnp.zeros((rows, 2 * rows), ref.dtype)
         side = 0 if first else rows
@@ -120,7 +119,7 @@
 
 def pack(after, tok_t, ffn_gain, splits):
     width, rows = tok_t.shape
-    lanes = len(splits) * half_of(splits[0].shape[1]) + rows + 2 * width
+    lanes = sum(widths(splits[0].shape[1])[1:]) + rows + 2 * width
     arrays = (after, tok_t, ffn_gain, *splits)
     return pl.pallas_call(
         pack_kernel,
@@ -195,11 +194,11 @@
     )(in_vmem(parts))
 
 
-def widen_kernel(parts, mine, got, _, out_ref, mid_ref):
+def widen_kernel(parts, mine, got, _, out_ref, mid_ref, *, alone):
     r = member(lax.axis_index("kv"))
     _, seqs = mid_ref.shape
-    half = out_ref.shape[1] // 2
-    end = 3 * half
+    both = out_ref.shape[-1]
+    end = both + alone
 
     def mid_of(ref, at):
         return (ref[:, end : end + seqs].astype(jnp.float32) + parts[at]).astype(jnp.bfloat16)
@@ -210,21 +209,22 @@
     gains = mine[0:1, end + seqs :].astype(jnp.float32) + got[0:1, end + seqs :].astype(jnp.float32)
     ffn_in = (x * gains).astype(jnp.bfloat16)
     squares = jnp.sum(x * x, axis=1, keepdims=True)
-    weights = jnp.concatenate([mine[:, : 2 * half], got[:, : 2 * half]], axis=0)
+    weights = jnp.concatenate([mine[:, :both], got[:, :both]], axis=0)
     made = jnp.dot(ffn_in, weights, preferred_element_type=jnp.float32)
     lane = lax.broadcasted_iota(jnp.int32, (seqs, 128), 1)
     out_ref[...] = made.astype(jnp.bfloat16)
-    out_ref[:, half - 128 : half] = jnp.where(lane == 127, squares, made[:, half - 128 : half]).astype(
+    out_ref[:, both - 128 :] = jnp.where(lane == 127, squares, made[:, both - 128 :]).astype(
         jnp.bfloat16
     )
 
 
-def widen(parts, mine, got, new_state, half):
+def widen(parts, mine, got, new_state, units):
     width, seqs = parts.shape[1:]
-    return pl.pallas_call(
-        widen_kernel,
+    _, both, alone = widths(units)
+    return pl.pallas_call(
+        functools.partial(widen_kernel, alone=alone),
         out_shape=(
-            pltpu.VMEM((seqs, 2 * half), jnp.bfloat16),
+            pltpu.VMEM((seqs, both), jnp.bfloat16),
             pltpu.VMEM((width, seqs), jnp.bfloat16),
         ),
         in_specs=whole(4),
@@ -234,13 +234,36 @@
     )(*(in_vmem(a) for a in (parts, mine, got, new_state)))
 
 
-def narrow_kernel(hidden, mine, got, out_ref):
+def gate_kernel(sums, out_ref, *, half, model_width):
+    rows, both = sums.shape
+    alone = out_ref.shape[-1]
+    rms = lax.rsqrt(sums[:, both - 1 :] / model_width + epsilon)
+    gate = sums[:, :half] * rms
+    up = sums[:, half : 2 * half] * rms
+    hidden = gate / (1.0 + jnp.exp(-gate)) * up
+    filled = jnp.concatenate([hidden, jnp.zeros((rows, alone - half), jnp.float32)], axis=1)
+    out_ref[...] = jnp.broadcast_to(filled.astype(jnp.bfloat16)[None], out_ref.shape)
+
+
+def gate_units(sums, units, model_width, copies):
+    half, _, alone = widths(units)
+    return pl.pallas_call(
+        functools.partial(gate_kernel, half=half, model_width=model_width),
+        out_shape=pltpu.VMEM((copies, sums.shape[0], alone), jnp.bfloat16),
+        in_specs=whole(1),
+        out_specs=pl.BlockSpec(memory_space=pltpu.VMEM),
+        compiler_params=pltpu.CompilerParams(vmem_limit_bytes=8 << 20),
+        name="gate",
+    )(in_vmem(sums))
+
+
+def narrow_kernel(hidden, mine, got, out_ref, *, both):
     r = member(lax.axis_index("kv"))
-    half = hidden.shape[1]
+    alone = hidden.shape[1]
     copies, _ = out_ref.shape[1:3]
     for ref, at in ((mine, r), (got, 1 - r)):
         made = lax.dot_general(
-            ref[:, 2 * half : 3 * half],
+            ref[:, both : both + alone],
             hidden[...],
             (((1,), (1,)), ((), ())),
             preferred_element_type=jnp.float32,
@@ -249,10 +272,10 @@
             out_ref[at, j] = made
 
 
-def narrow(hidden, mine, got, tp):
+def narrow(hidden, mine, got, units, tp):
     width, seqs = (mine.shape[0], hidden.shape[0])
     return pl.pallas_call(
-        narrow_kernel,
+        functools.partial(narrow_kernel, both=widths(units)[1]),
         out_shape=pltpu.VMEM((2, tp, width, seqs), jnp.bfloat16),
         in_specs=whole(3),
         out_specs=pl.BlockSpec(memory_space=pltpu.VMEM),
@@ -315,16 +338,13 @@
     width, seqs = attn_part.shape
     pair, line = (pairs(kv, tp), lines(kv))
     attn_parts = exchanged(copies_of(attn_part, 2 * tp), ("kv", "tp"), pair)
-    half = half_of(w_ffgate.shape[1])
+    units = w_ffgate.shape[1]
     attn_sums = total(attn_parts.reshape(2, tp, width, seqs))
-    wide, mid_t = widen(attn_sums, mine, got, new_state, half)
+    wide, mid_t = widen(attn_sums, mine, got, new_state, units)
     count = len(line[0])
     sums = summed(exchanged(wide.reshape(count, seqs // count, -1), "kv", line))
-    ffn_rms = lax.rsqrt(sums[:, half - 1 : half] / model_width + epsilon)
-    gated = jax.nn.silu(sums[:, :half] * ffn_rms) * (sums[:, half:] * ffn_rms)
-    hidden = gated.astype(jnp.bfloat16)
-    hidden_all = exchanged(copies_of(hidden, count), "kv", line).reshape(seqs, half)
-    down_parts = narrow(hidden_all, mine, got, tp).reshape(2 * tp, width, seqs)
+    hidden = exchanged(gate_units(sums, units, model_width, count), "kv", line)
+    down_parts = narrow(hidden.reshape(seqs, -1), mine, got, units, tp).reshape(2 * tp, width, seqs)
     mixed = (
         mid_t.astype(jnp.float32) + summed(exchanged(down_parts, ("kv", "tp"), pair))
     ).astype(jnp.bfloat16)

time: 128 us -> 127 us (level)
  no operation moved by 1% of the time
where the time goes in v6:
time: 127 us; the launch traced here: 126 us
  blocking collectives  81.9 us (64%)
  waiting for transfers between devices  19.5 us (15%)
  starting transfers between devices  17.3 us (14%)
  Pallas kernels  3.24 us (3%)
  local copies, waits for them, and re-layouts  1.91 us (2%)
  other arithmetic  1.44 us (1%)
    all_to_all x4, blocking collectives, exchanged(): lax.all_to_all(blocks, axis, 0, 0, axis_index_groups=groups, tiled=True)  81.9 us
    all_to_all x2, waiting for transfers between devices, exchanged(): lax.all_to_all(blocks, axis, 0, 0, axis_index_groups=groups, tiled=True)  15.1 us
    all_to_all x2, starting transfers between devices, exchanged(): lax.all_to_all(blocks, axis, 0, 0, axis_index_groups=groups, tiled=True)  14 us
    ppermute x1, waiting for transfers between devices, local(): got = lax.ppermute(sent, 'kv', [(i, i ^ 1) for i in range(kv)])  4.43 us
    ppermute x1, starting transfers between devices, local(): got = lax.ppermute(sent, 'kv', [(i, i ^ 1) for i in range(kv)])  3.26 us
  transfers between devices with their start and end apart: 3, of which 3 were waited for; matrix products, arithmetic and copies ran while one was open for 0% of the time, Pallas kernels for 0%

profile of v6, /device:TPU:1, one launch (start us, length us, event | category | flops | bytes accessed | tf_op | source)
XLA Modules:
  0.0 126.3 jit_solution(13627320821101244887)
XLA Ops:
  0.6 0.0 copy-start
  0.6 1.8 %project.1 = (bf16[128,1920]{1,0:T(8,128)(2,1)S(1)}, f32[1,256]{1,0:T(1,128)S(1)}, bf16[4,128]{1,0:T(4,128)(2,1)S(1)}, bf16[1,64]{1,0:T(2,128)(2,1)S(1)}) custom-call(bf16[64,128]{1,0:T(8,128)(2,1)} %bitcast.17, bf16[1,64]{1,0:T(2,128)(2,1)} %bitcast.21, bf16[64,256]{1,0:T(8,128)(2,1)} %refs_2_.1, bf16[64,256]{1,0:T(8,128)(2,1)} %refs_3_.1, ...), custom_call_target="tpu_custom_call" | custom-call | tf_op jit(solution)/shard_map/project/pallas_call | solution.py:79
  2.5 0.0 copy-start.1
  2.5 0.2 reshape.41
  2.7 33.8 %all_to_all.30 = bf16[64,2,1920]{2,1,0:T(2,128)(2,1)S(1)} all-to-all(bf16[64,2,1920]{2,1,0:T(2,128)(2,1)S(1)} %reshape.41), channel_id=1, replica_groups=mesh['kv'=64,'tp'=8] {'kv'}, dimensions={0} | all-to-all | bytes 983040 | tf_op jit(solution)/shard_map/all_to_all | solution.py:288
  36.5 0.4 convert_reduce_fusion.sums
  36.9 0.0 copy-done.1
  36.9 0.5 attend.1
  37.4 0.7 broadcast_in_dim.13
  38.1 6.5 %all-to-all-start.1 = ((bf16[64,2,512]{2,1,0:T(2,128)(2,1)}), bf16[64,2,512]{2,1,0:T(2,128)(2,1)S(1)}, u32[]{:S(2)}, u32[]{:S(2)}) async-start(bf16[64,2,512]{2,1,0:T(2,128)(2,1)} %broadcast_in_dim.13), calls=%async_computation.1 | async-start | bytes 262144 | tf_op jit(solution)/shard_map/all_to_all | solution.py:288
  44.6 0.2 multiply_add_fusion._
  44.8 0.0 copy-start.2
  44.9 11.3 %all-to-all-done.1 = bf16[64,2,512]{2,1,0:T(2,128)(2,1)S(1)} async-done(((bf16[64,2,512]{2,1,0:T(2,128)(2,1)}), bf16[64,2,512]{2,1,0:T(2,128)(2,1)S(1)}, u32[]{:S(2)}, u32[]{:S(2)}) %all-to-all-start.1) | async-done | bytes 131104 | tf_op jit(solution)/shard_map/all_to_all | solution.py:288
  56.2 0.1 reshape.42
  56.2 0.0 copy-done
  56.3 0.2 fusion
  56.4 0.0 copy-start.5
  56.4 0.8 broadcast_in_dim.28
  57.2 0.0 copy-start.3
  57.2 0.0 copy-start.4
  57.2 0.0 copy-start.6
  57.2 7.5 %all-to-all-start.2 = ((bf16[16,64,128]{2,1,0:T(8,128)(2,1)}), bf16[16,64,128]{2,1,0:T(8,128)(2,1)S(1)}, u32[]{:S(2)}, u32[]{:S(2)}) async-start(bf16[16,64,128]{2,1,0:T(8,128)(2,1)} %broadcast_in_dim.28), calls=%async_computation.2 | async-start | bytes 524288 | tf_op jit(solution)/shard_map/all_to_all | solution.py:288
  64.7 0.0 copy-done.5
  64.7 0.0 copy-done.3
  64.7 0.0 copy-done.4
  64.7 0.0 copy-done.6
  64.8 0.2 pack.1
  64.9 3.3 %collective-permute-start = (bf16[64,2432]{1,0:T(8,128)(2,1)S(1)}, bf16[64,2432]{1,0:T(8,128)(2,1)S(1)}, u32[]{:S(2)}, u32[]{:S(2)}) collective-permute-start(bf16[64,2432]{1,0:T(8,128)(2,1)S(1)} %get-tuple-element.26), channel_id=1, source_target_pairs={{0,8},{8,0},{16,24},{24,16},{32,40},{40,32},{48,56},{56,48},{64,72... | collective-permute-start | bytes 933896 | tf_op jit(solution)/shard_map/ppermute | solution.py:329
  68.2 3.8 %all-to-all-done.2 = bf16[16,64,128]{2,1,0:T(8,128)(2,1)S(1)} async-done(((bf16[16,64,128]{2,1,0:T(8,128)(2,1)}), bf16[16,64,128]{2,1,0:T(8,128)(2,1)S(1)}, u32[]{:S(2)}, u32[]{:S(2)}) %all-to-all-start.2) | async-done | bytes 262176 | tf_op jit(solution)/shard_map/all_to_all | solution.py:288
  72.0 4.4 %collective-permute-done.got = bf16[64,2432]{1,0:T(8,128)(2,1)S(1)} collective-permute-done((bf16[64,2432]{1,0:T(8,128)(2,1)S(1)}, bf16[64,2432]{1,0:T(8,128)(2,1)S(1)}, u32[]{:S(2)}, u32[]{:S(2)}) %collective-permute-start) | collective-permute-done | bytes 311328 | tf_op jit(solution)/shard_map/ppermute | solution.py:329
  76.4 0.0 copy-done.2
  76.4 0.3 widen.1
  76.8 0.1 reshape.44
  76.9 17.3 %all_to_all.31 = bf16[32,4,1408]{2,1,0:T(4,128)(2,1)S(1)} all-to-all(bf16[32,4,1408]{2,1,0:T(4,128)(2,1)S(1)} %reshape.44), channel_id=1, replica_groups={{0,16,40,56,64,80,104,120,128,144,168,184,192,208,232,248,256,272,296,3..., dimensions={0} | all-to-all | bytes 720896 | tf_op jit(solution)/shard_map/all_to_all | solution.py:288
  94.1 0.2 convert_reduce_fusion.1.sums
  94.3 0.2 gate.1
  94.4 15.5 %all_to_all.32 = bf16[32,4,768]{2,1,0:T(4,128)(2,1)S(1)} all-to-all(bf16[32,4,768]{2,1,0:T(4,128)(2,1)S(1)} %gate.1), channel_id=1, replica_groups={{0,16,40,56,64,80,104,120,128,144,168,184,192,208,232,248,256,272,296,3..., dimensions={0} | all-to-all | bytes 393216 | tf_op jit(solution)/shard_map/all_to_all | solution.py:288
  109.9 0.1 reshape.45.hidden
  110.0 0.3 narrow.1
  110.2 15.4 %all_to_all.33 = bf16[16,64,128]{2,1,0:T(8,128)(2,1)S(1)} all-to-all(bf16[16,64,128]{2,1,0:T(8,128)(2,1)S(1)} %bitcast.15), channel_id=1, replica_groups={{0,1,2,3,4,5,6,7,8,9,10,11,12,13,14,15},{16,17,18,19,20,21,22,23,24,25,..., dimensions={0} | all-to-all | bytes 524288 | tf_op jit(solution)/shard_map/all_to_all | solution.py:288
  125.7 0.6 fusion.1
  (2 shorter events, 0.1 us)
Async XLA Ops:
  0.6 55.6 %copy-start = (bf16[512,64]{0,1:T(8,128)(2,1)S(1)}, bf16[512,64]{0,1:T(8,128)(2,1)}, u32[]{:S(2)}) copy-start(bf16[512,64]{0,1:T(8,128)(2,1)} %param.25) | copy-start | bytes 196612
  2.5 34.4 %copy-start.1 = (f32[2,1,256,512]{3,2,1,0:T(8,128)S(1)}, f32[2,1,256,512]{3,2,1,0:T(8,128)}, u32[]{:S(2)}) copy-start(f32[2,1,256,512]{3,2,1,0:T(8,128)} %state.1) | copy-start | bytes 3145732
  38.1 18.0 %all-to-all-start.1 = ((bf16[64,2,512]{2,1,0:T(2,128)(2,1)}), bf16[64,2,512]{2,1,0:T(2,128)(2,1)S(1)}, u32[]{:S(2)}, u32[]{:S(2)}) async-start(bf16[64,2,512]{2,1,0:T(2,128)(2,1)} %broadcast_in_dim.13), calls=%async_computation.1 | async-start | bytes 262144 | tf_op jit(solution)/shard_map/all_to_all | solution.py:288
  44.8 31.6 %copy-start.2 = (f32[2,1,256,512]{3,2,1,0:T(8,128)}, f32[2,1,256,512]{3,2,1,0:T(8,128)S(1)}, u32[]{:S(2)}) copy-start(f32[2,1,256,512]{3,2,1,0:T(8,128)S(1)} %multiply_add_fusion._) | copy-start | bytes 3145732
  56.4 8.3 %copy-start.5 = (bf16[1376,64]{0,1:T(8,128)(2,1)S(1)}, bf16[1376,64]{0,1:T(8,128)(2,1)}, u32[]{:S(2)}) copy-start(bf16[1376,64]{0,1:T(8,128)(2,1)} %param.28) | copy-start | bytes 528388
  57.2 7.5 %copy-start.3 = (bf16[64,1376]{1,0:T(8,128)(2,1)S(1)}, bf16[64,1376]{1,0:T(8,128)(2,1)}, u32[]{:S(2)}) copy-start(bf16[64,1376]{1,0:T(8,128)(2,1)} %refs_0_.1) | copy-start | bytes 528388
  57.2 7.6 %copy-start.4 = (bf16[64,1376]{1,0:T(8,128)(2,1)S(1)}, bf16[64,1376]{1,0:T(8,128)(2,1)}, u32[]{:S(2)}) copy-start(bf16[64,1376]{1,0:T(8,128)(2,1)} %refs_1_.1) | copy-start | bytes 528388
  57.2 7.6 %copy-start.6 = (bf16[128,64]{0,1:T(8,128)(2,1)S(1)}, bf16[128,64]{0,1:T(8,128)(2,1)}, u32[]{:S(2)}) copy-start(bf16[128,64]{0,1:T(8,128)(2,1)} %param.15) | copy-start | bytes 49156
  57.2 14.8 %all-to-all-start.2 = ((bf16[16,64,128]{2,1,0:T(8,128)(2,1)}), bf16[16,64,128]{2,1,0:T(8,128)(2,1)S(1)}, u32[]{:S(2)}, u32[]{:S(2)}) async-start(bf16[16,64,128]{2,1,0:T(8,128)(2,1)} %broadcast_in_dim.28), calls=%async_computation.2 | async-start | bytes 524288 | tf_op jit(solution)/shard_map/all_to_all | solution.py:288
  64.9 11.5 %collective-permute-start = (bf16[64,2432]{1,0:T(8,128)(2,1)S(1)}, bf16[64,2432]{1,0:T(8,128)(2,1)S(1)}, u32[]{:S(2)}, u32[]{:S(2)}) collective-permute-start(bf16[64,2432]{1,0:T(8,128)(2,1)S(1)} %get-tuple-element.26), channel_id=1, source_target_pairs={{0,8},{8,0},{16,24},{24,16},{32,40},{40,32},{48,56},{56,48},{64,72... | collective-permute-start | bytes 933896 | tf_op jit(solution)/shard_map/ppermute | solution.py:329

commit v7 on v6

--- a/solution.py
+++ b/solution.py
@@ -64,22 +64,23 @@
         copy.wait()
         n = w.shape[1]
         part = jnp.dot(mix_in, w[...], preferred_element_type=jnp.float32)
-        out_ref[:, at : at + n] = part.astype(jnp.bfloat16)
+        out_ref[..., at : at + n] = part.reshape(*out_ref.shape[:2], n).astype(jnp.bfloat16)
         at += n
-    rest = out_ref.shape[1] - at
+    rest = out_ref.shape[2] - at
     lane = lax.broadcasted_iota(jnp.int32, (x.shape[0], rest), 1)
-    out_ref[:, at:] = jnp.where(lane == 0, squares, 0.0).astype(jnp.bfloat16)
+    last = jnp.where(lane == 0, squares, 0.0)
+    out_ref[..., at:] = last.reshape(*out_ref.shape[:2], rest).astype(jnp.bfloat16)
     for copy in copies[count - kept :]:
         copy.wait()
 
 
-def project(tok_t, gain, weights, kept):
+def project(tok_t, gain, weights, kept, count):
     total = sum(w.shape[1] for w in weights)
     arrays = (tok_t, gain, *weights, *kept)
     return pl.pallas_call(
         functools.partial(project_kernel, count=len(arrays), kept=len(kept)),
         out_shape=(
-            pltpu.VMEM((tok_t.shape[1], total + 128), jnp.bfloat16),
+            pltpu.VMEM((count, tok_t.shape[1] // count, total + 128), jnp.bfloat16),
             *(pltpu.VMEM(a.shape, a.dtype) for a in kept),
         ),
         in_specs=[pl.BlockSpec(memory_space=pl.ANY)] * len(arrays),
@@ -212,19 +213,18 @@
     weights = jnp.concatenate([mine[:, :both], got[:, :both]], axis=0)
     made = jnp.dot(ffn_in, weights, preferred_element_type=jnp.float32)
     lane = lax.broadcasted_iota(jnp.int32, (seqs, 128), 1)
-    out_ref[...] = made.astype(jnp.bfloat16)
-    out_ref[:, both - 128 :] = jnp.where(lane == 127, squares, made[:, both - 128 :]).astype(
-        jnp.bfloat16
-    )
-
-
-def widen(parts, mine, got, new_state, units):
+    last = jnp.where(lane == 127, squares, made[:, both - 128 :])
+    made = jnp.concatenate([made[:, : both - 128], last], axis=1)
+    out_ref[...] = made.reshape(out_ref.shape).astype(jnp.bfloat16)
+
+
+def widen(parts, mine, got, new_state, units, count):
     width, seqs = parts.shape[1:]
     _, both, alone = widths(units)
     return pl.pallas_call(
         functools.partial(widen_kernel, alone=alone),
         out_shape=(
-            pltpu.VMEM((seqs, both), jnp.bfloat16),
+            pltpu.VMEM((count, seqs // count, both), jnp.bfloat16),
             pltpu.VMEM((width, seqs), jnp.bfloat16),
         ),
         in_specs=whole(4),
@@ -313,7 +313,7 @@
     w_down,
     state,
 ):
-    own_rows, heads, _, val_dim = state.shape
+    _, heads, _, val_dim = state.shape
     kv, tp = (lax.axis_size(a) for a in ("kv", "tp"))
     model_width = tokens.shape[1] * kv
     made, bias, head_scale, ffn_scale = project(
@@ -321,8 +321,9 @@
         mix_gain[None, :],
         (w_query, w_key, w_value, w_gate, w_decay),
         (decay_bias[None, :], head_gain.reshape(-1, 128), ffn_gain[None, :]),
+        kv,
     )
-    arrived = exchanged(made.reshape(kv, own_rows, -1), "kv")
+    arrived = exchanged(made, "kv")
     keys, values, decay, head_out = attend(summed(arrived), bias, head_scale, state, model_width)
     heads_all = exchanged(copies_of(head_out, kv), "kv")
     mine, sent = pack(head_out, tokens.T, ffn_scale, (w_ffgate, w_ffup, w_down.T))
@@ -340,9 +341,9 @@
     attn_parts = exchanged(copies_of(attn_part, 2 * tp), ("kv", "tp"), pair)
     units = w_ffgate.shape[1]
     attn_sums = total(attn_parts.reshape(2, tp, width, seqs))
-    wide, mid_t = widen(attn_sums, mine, got, new_state, units)
     count = len(line[0])
-    sums = summed(exchanged(wide.reshape(count, seqs // count, -1), "kv", line))
+    wide, mid_t = widen(attn_sums, mine, got, new_state, units, count)
+    sums = summed(exchanged(wide, "kv", line))
     hidden = exchanged(gate_units(sums, units, model_width, count), "kv", line)
     down_parts = narrow(hidden.reshape(seqs, -1), mine, got, units, tp).reshape(2 * tp, width, seqs)
     mixed = (

time: 127 us -> 127 us (level)
  no operation moved by 1% of the time
where the time goes in v7:
time: 127 us; the launch traced here: 126 us
  blocking collectives  81.8 us (64%)
  waiting for transfers between devices  19.5 us (15%)
  starting transfers between devices  17.3 us (14%)
  Pallas kernels  3.57 us (3%)
  local copies, waits for them, and re-layouts  1.63 us (1%)
  other arithmetic  1.44 us (1%)
    all_to_all x4, blocking collectives, exchanged(): lax.all_to_all(blocks, axis, 0, 0, axis_index_groups=groups, tiled=True)  81.8 us
    all_to_all x2, waiting for transfers between devices, exchanged(): lax.all_to_all(blocks, axis, 0, 0, axis_index_groups=groups, tiled=True)  15.1 us
    all_to_all x2, starting transfers between devices, exchanged(): lax.all_to_all(blocks, axis, 0, 0, axis_index_groups=groups, tiled=True)  14 us
    ppermute x1, waiting for transfers between devices, local(): got = lax.ppermute(sent, 'kv', [(i, i ^ 1) for i in range(kv)])  4.43 us
    ppermute x1, starting transfers between devices, local(): got = lax.ppermute(sent, 'kv', [(i, i ^ 1) for i in range(kv)])  3.26 us
  transfers between devices with their start and end apart: 3, of which 3 were waited for; matrix products, arithmetic and copies ran while one was open for 0% of the time, Pallas kernels for 0%

profile of v7, /device:TPU:1, one launch (start us, length us, event | category | flops | bytes accessed | tf_op | source)
XLA Modules:
  0.0 126.2 jit_solution(13579193047053513907)
XLA Ops:
  0.6 0.0 copy-start
  0.6 0.0 copy-start.1
  0.7 2.1 %project.1 = (bf16[64,2,1920]{2,1,0:T(2,128)(2,1)S(1)}, f32[1,256]{1,0:T(1,128)S(1)}, bf16[4,128]{1,0:T(4,128)(2,1)S(1)}, bf16[1,64]{1,0:T(2,128)(2,1)S(1)}) custom-call(bf16[64,128]{1,0:T(8,128)(2,1)} %bitcast.17, bf16[1,64]{1,0:T(2,128)(2,1)} %bitcast.21, bf16[64,256]{1,0:T(8,128)(2,1)} %refs_2_.1, bf16[64,256]{1,0:T(8,128)(2,1)} %refs_3_.1, ...), custom_call_target="tpu_custom_call" | custom-call | tf_op jit(solution)/shard_map/project/pallas_call | solution.py:80
  2.8 33.7 %all_to_all.30 = bf16[64,2,1920]{2,1,0:T(2,128)(2,1)S(1)} all-to-all(bf16[64,2,1920]{2,1,0:T(2,128)(2,1)S(1)} %get-tuple-element.16), channel_id=1, replica_groups=mesh['kv'=64,'tp'=8] {'kv'}, dimensions={0} | all-to-all | bytes 983040 | tf_op jit(solution)/shard_map/all_to_all | solution.py:288
  36.5 0.4 convert_reduce_fusion.sums
  36.9 0.0 copy-done.1
  36.9 0.5 attend.1
  37.4 0.7 broadcast_in_dim.13
  38.1 6.5 %all-to-all-start.1 = ((bf16[64,2,512]{2,1,0:T(2,128)(2,1)}), bf16[64,2,512]{2,1,0:T(2,128)(2,1)S(1)}, u32[]{:S(2)}, u32[]{:S(2)}) async-start(bf16[64,2,512]{2,1,0:T(2,128)(2,1)} %broadcast_in_dim.13), calls=%async_computation.1 | async-start | bytes 262144 | tf_op jit(solution)/shard_map/all_to_all | solution.py:288
  44.6 0.2 multiply_add_fusion._
  44.8 0.0 copy-start.2
  44.8 11.3 %all-to-all-done.1 = bf16[64,2,512]{2,1,0:T(2,128)(2,1)S(1)} async-done(((bf16[64,2,512]{2,1,0:T(2,128)(2,1)}), bf16[64,2,512]{2,1,0:T(2,128)(2,1)S(1)}, u32[]{:S(2)}, u32[]{:S(2)}) %all-to-all-start.1) | async-done | bytes 131104 | tf_op jit(solution)/shard_map/all_to_all | solution.py:288
  56.2 0.1 reshape.35
  56.2 0.0 copy-done
  56.2 0.2 fusion
  56.4 0.0 copy-start.5
  56.4 0.8 broadcast_in_dim.28
  57.2 0.0 copy-start.3
  57.2 0.0 copy-start.4
  57.2 0.0 copy-start.6
  57.2 7.5 %all-to-all-start.2 = ((bf16[16,64,128]{2,1,0:T(8,128)(2,1)}), bf16[16,64,128]{2,1,0:T(8,128)(2,1)S(1)}, u32[]{:S(2)}, u32[]{:S(2)}) async-start(bf16[16,64,128]{2,1,0:T(8,128)(2,1)} %broadcast_in_dim.28), calls=%async_computation.2 | async-start | bytes 524288 | tf_op jit(solution)/shard_map/all_to_all | solution.py:288
  64.7 0.0 copy-done.5
  64.7 0.0 copy-done.3
  64.7 0.0 copy-done.4
  64.7 0.0 copy-done.6
  64.7 0.2 pack.1
  64.9 3.3 %collective-permute-start = (bf16[64,2432]{1,0:T(8,128)(2,1)S(1)}, bf16[64,2432]{1,0:T(8,128)(2,1)S(1)}, u32[]{:S(2)}, u32[]{:S(2)}) collective-permute-start(bf16[64,2432]{1,0:T(8,128)(2,1)S(1)} %get-tuple-element.26), channel_id=1, source_target_pairs={{0,8},{8,0},{16,24},{24,16},{32,40},{40,32},{48,56},{56,48},{64,72... | collective-permute-start | bytes 933896 | tf_op jit(solution)/shard_map/ppermute | solution.py:330
  68.2 3.8 %all-to-all-done.2 = bf16[16,64,128]{2,1,0:T(8,128)(2,1)S(1)} async-done(((bf16[16,64,128]{2,1,0:T(8,128)(2,1)}), bf16[16,64,128]{2,1,0:T(8,128)(2,1)S(1)}, u32[]{:S(2)}, u32[]{:S(2)}) %all-to-all-start.2) | async-done | bytes 262176 | tf_op jit(solution)/shard_map/all_to_all | solution.py:288
  72.0 4.4 %collective-permute-done.got = bf16[64,2432]{1,0:T(8,128)(2,1)S(1)} collective-permute-done((bf16[64,2432]{1,0:T(8,128)(2,1)S(1)}, bf16[64,2432]{1,0:T(8,128)(2,1)S(1)}, u32[]{:S(2)}, u32[]{:S(2)}) %collective-permute-start) | collective-permute-done | bytes 311328 | tf_op jit(solution)/shard_map/ppermute | solution.py:330
  76.4 0.0 copy-done.2
  76.4 0.3 widen.1
  76.8 17.2 %all_to_all.31 = bf16[32,4,1408]{2,1,0:T(4,128)(2,1)S(1)} all-to-all(bf16[32,4,1408]{2,1,0:T(4,128)(2,1)S(1)} %get-tuple-element.29), channel_id=1, replica_groups={{0,16,40,56,64,80,104,120,128,144,168,184,192,208,232,248,256,272,296,3..., dimensions={0} | all-to-all | bytes 720896 | tf_op jit(solution)/shard_map/all_to_all | solution.py:288
  94.0 0.2 convert_reduce_fusion.1.sums
  94.2 0.2 gate.1
  94.3 15.5 %all_to_all.32 = bf16[32,4,768]{2,1,0:T(4,128)(2,1)S(1)} all-to-all(bf16[32,4,768]{2,1,0:T(4,128)(2,1)S(1)} %gate.1), channel_id=1, replica_groups={{0,16,40,56,64,80,104,120,128,144,168,184,192,208,232,248,256,272,296,3..., dimensions={0} | all-to-all | bytes 393216 | tf_op jit(solution)/shard_map/all_to_all | solution.py:288
  109.8 0.1 reshape.37.hidden
  109.9 0.3 narrow.1
  110.2 15.4 %all_to_all.33 = bf16[16,64,128]{2,1,0:T(8,128)(2,1)S(1)} all-to-all(bf16[16,64,128]{2,1,0:T(8,128)(2,1)S(1)} %bitcast.15), channel_id=1, replica_groups={{0,1,2,3,4,5,6,7,8,9,10,11,12,13,14,15},{16,17,18,19,20,21,22,23,24,25,..., dimensions={0} | all-to-all | bytes 524288 | tf_op jit(solution)/shard_map/all_to_all | solution.py:288
  125.6 0.6 fusion.1
  (2 shorter events, 0.1 us)
Async XLA Ops:
  0.6 55.6 %copy-start = (bf16[512,64]{0,1:T(8,128)(2,1)S(1)}, bf16[512,64]{0,1:T(8,128)(2,1)}, u32[]{:S(2)}) copy-start(bf16[512,64]{0,1:T(8,128)(2,1)} %param.25) | copy-start | bytes 196612
  0.6 36.2 %copy-start.1 = (f32[2,1,256,512]{3,2,1,0:T(8,128)S(1)}, f32[2,1,256,512]{3,2,1,0:T(8,128)}, u32[]{:S(2)}) copy-start(f32[2,1,256,512]{3,2,1,0:T(8,128)} %state.1) | copy-start | bytes 3145732
  38.1 18.0 %all-to-all-start.1 = ((bf16[64,2,512]{2,1,0:T(2,128)(2,1)}), bf16[64,2,512]{2,1,0:T(2,128)(2,1)S(1)}, u32[]{:S(2)}, u32[]{:S(2)}) async-start(bf16[64,2,512]{2,1,0:T(2,128)(2,1)} %broadcast_in_dim.13), calls=%async_computation.1 | async-start | bytes 262144 | tf_op jit(solution)/shard_map/all_to_all | solution.py:288
  44.8 31.6 %copy-start.2 = (f32[2,1,256,512]{3,2,1,0:T(8,128)}, f32[2,1,256,512]{3,2,1,0:T(8,128)S(1)}, u32[]{:S(2)}) copy-start(f32[2,1,256,512]{3,2,1,0:T(8,128)S(1)} %multiply_add_fusion._) | copy-start | bytes 3145732
  56.4 8.3 %copy-start.5 = (bf16[1376,64]{0,1:T(8,128)(2,1)S(1)}, bf16[1376,64]{0,1:T(8,128)(2,1)}, u32[]{:S(2)}) copy-start(bf16[1376,64]{0,1:T(8,128)(2,1)} %param.28) | copy-start | bytes 528388
  57.2 7.6 %copy-start.3 = (bf16[64,1376]{1,0:T(8,128)(2,1)S(1)}, bf16[64,1376]{1,0:T(8,128)(2,1)}, u32[]{:S(2)}) copy-start(bf16[64,1376]{1,0:T(8,128)(2,1)} %refs_0_.1) | copy-start | bytes 528388
  57.2 7.6 %copy-start.4 = (bf16[64,1376]{1,0:T(8,128)(2,1)S(1)}, bf16[64,1376]{1,0:T(8,128)(2,1)}, u32[]{:S(2)}) copy-start(bf16[64,1376]{1,0:T(8,128)(2,1)} %refs_1_.1) | copy-start | bytes 528388
  57.2 7.6 %copy-start.6 = (bf16[128,64]{0,1:T(8,128)(2,1)S(1)}, bf16[128,64]{0,1:T(8,128)(2,1)}, u32[]{:S(2)}) copy-start(bf16[128,64]{0,1:T(8,128)(2,1)} %param.15) | copy-start | bytes 49156
  57.2 14.8 %all-to-all-start.2 = ((bf16[16,64,128]{2,1,0:T(8,128)(2,1)}), bf16[16,64,128]{2,1,0:T(8,128)(2,1)S(1)}, u32[]{:S(2)}, u32[]{:S(2)}) async-start(bf16[16,64,128]{2,1,0:T(8,128)(2,1)} %broadcast_in_dim.28), calls=%async_computation.2 | async-start | bytes 524288 | tf_op jit(solution)/shard_map/all_to_all | solution.py:288
  64.9 11.5 %collective-permute-start = (bf16[64,2432]{1,0:T(8,128)(2,1)S(1)}, bf16[64,2432]{1,0:T(8,128)(2,1)S(1)}, u32[]{:S(2)}, u32[]{:S(2)}) collective-permute-start(bf16[64,2432]{1,0:T(8,128)(2,1)S(1)} %get-tuple-element.26), channel_id=1, source_target_pairs={{0,8},{8,0},{16,24},{24,16},{32,40},{40,32},{48,56},{56,48},{64,72... | collective-permute-start | bytes 933896 | tf_op jit(solution)/shard_map/ppermute | solution.py:330

commit v8 on v6

--- a/solution.py
+++ b/solution.py
@@ -179,6 +179,25 @@
     )(*(in_vmem(a) for a in (sums, bias, gain, state)))
 
 
+def join_kernel(heads, weights, out_ref):
+    made = lax.dot_general(
+        weights[...], heads[...], (((1,), (1,)), ((), ())), preferred_element_type=jnp.float32
+    ).astype(jnp.bfloat16)
+    for j in range(out_ref.shape[0]):
+        out_ref[j] = made
+
+
+def join(heads, weights, copies):
+    return pl.pallas_call(
+        join_kernel,
+        out_shape=pltpu.VMEM((copies, weights.shape[0], heads.shape[0]), jnp.bfloat16),
+        in_specs=whole(2),
+        out_specs=pl.BlockSpec(memory_space=pltpu.VMEM),
+        compiler_params=pltpu.CompilerParams(vmem_limit_bytes=8 << 20),
+        name="join",
+    )(*(in_vmem(a) for a in (heads, weights)))
+
+
 def total_kernel(parts, out_ref):
     out_ref[...] = jnp.sum(parts[...].astype(jnp.float32), axis=1)
 
@@ -212,19 +231,18 @@
     weights = jnp.concatenate([mine[:, :both], got[:, :both]], axis=0)
     made = jnp.dot(ffn_in, weights, preferred_element_type=jnp.float32)
     lane = lax.broadcasted_iota(jnp.int32, (seqs, 128), 1)
-    out_ref[...] = made.astype(jnp.bfloat16)
-    out_ref[:, both - 128 :] = jnp.where(lane == 127, squares, made[:, both - 128 :]).astype(
-        jnp.bfloat16
-    )
-
-
-def widen(parts, mine, got, new_state, units):
+    last = jnp.where(lane == 127, squares, made[:, both - 128 :])
+    made = jnp.concatenate([made[:, : both - 128], last], axis=1)
+    out_ref[...] = made.reshape(out_ref.shape).astype(jnp.bfloat16)
+
+
+def widen(parts, mine, got, new_state, units, count):
     width, seqs = parts.shape[1:]
     _, both, alone = widths(units)
     return pl.pallas_call(
         functools.partial(widen_kernel, alone=alone),
         out_shape=(
-            pltpu.VMEM((seqs, both), jnp.bfloat16),
+            pltpu.VMEM((count, seqs // count, both), jnp.bfloat16),
             pltpu.VMEM((width, seqs), jnp.bfloat16),
         ),
         in_specs=whole(4),
@@ -260,16 +278,14 @@
 def narrow_kernel(hidden, mine, got, out_ref, *, both):
     r = member(lax.axis_index("kv"))
     alone = hidden.shape[1]
-    copies, _ = out_ref.shape[1:3]
-    for ref, at in ((mine, r), (got, 1 - r)):
-        made = lax.dot_general(
-            ref[:, both : both + alone],
-            hidden[...],
-            (((1,), (1,)), ((), ())),
-            preferred_element_type=jnp.float32,
-        ).astype(jnp.bfloat16)
-        for j in range(copies):
-            out_ref[at, j] = made
+    copies, width = out_ref.shape[1:3]
+    weights = jnp.concatenate([ref[:, both : both + alone] for ref in (mine, got)], axis=0)
+    made = lax.dot_general(
+        weights, hidden[...], (((1,), (1,)), ((), ())), preferred_element_type=jnp.float32
+    ).astype(jnp.bfloat16)
+    for j in range(copies):
+        out_ref[r, j] = made[:width]
+        out_ref[1 - r, j] = made[width:]
 
 
 def narrow(hidden, mine, got, units, tp):
@@ -331,18 +347,16 @@
         decay[:, None, :, None] * state + keys[:, None, :, None] * values[:, None, None, :]
     )
     heads_all = heads_all.reshape(-1, heads * val_dim)
-    attn_part = lax.dot_general(
-        w_output, heads_all, (((0,), (1,)), ((), ())), preferred_element_type=jnp.float32
-    ).astype(jnp.bfloat16)
-    attn_part, new_state = lax.optimization_barrier((attn_part, new_state))
-    width, seqs = attn_part.shape
+    attn_copies = join(heads_all, w_output.T, 2 * tp)
+    attn_copies, new_state = lax.optimization_barrier((attn_copies, new_state))
+    width, seqs = attn_copies.shape[1:]
     pair, line = (pairs(kv, tp), lines(kv))
-    attn_parts = exchanged(copies_of(attn_part, 2 * tp), ("kv", "tp"), pair)
+    attn_parts = exchanged(attn_copies, ("kv", "tp"), pair)
     units = w_ffgate.shape[1]
     attn_sums = total(attn_parts.reshape(2, tp, width, seqs))
-    wide, mid_t = widen(attn_sums, mine, got, new_state, units)
     count = len(line[0])
-    sums = summed(exchanged(wide.reshape(count, seqs // count, -1), "kv", line))
+    wide, mid_t = widen(attn_sums, mine, got, new_state, units, count)
+    sums = summed(exchanged(wide, "kv", line))
     hidden = exchanged(gate_units(sums, units, model_width, count), "kv", line)
     down_parts = narrow(hidden.reshape(seqs, -1), mine, got, units, tp).reshape(2 * tp, width, seqs)
     mixed = (

time: 127 us -> 127 us (level)
  no operation moved by 1% of the time
where the time goes in v8:
time: 127 us; the launch traced here: 126 us
  blocking collectives  81.9 us (64%)
  waiting for transfers between devices  19.5 us (15%)
  starting transfers between devices  17.3 us (14%)
  Pallas kernels  4.07 us (3%)
  other arithmetic  1.44 us (1%)
    all_to_all x4, blocking collectives, exchanged(): lax.all_to_all(blocks, axis, 0, 0, axis_index_groups=groups, tiled=True)  81.9 us
    all_to_all x2, waiting for transfers between devices, exchanged(): lax.all_to_all(blocks, axis, 0, 0, axis_index_groups=groups, tiled=True)  15.1 us
    all_to_all x2, starting transfers between devices, exchanged(): lax.all_to_all(blocks, axis, 0, 0, axis_index_groups=groups, tiled=True)  14 us
    ppermute x1, waiting for transfers between devices, local(): got = lax.ppermute(sent, 'kv', [(i, i ^ 1) for i in range(kv)])  4.43 us
    ppermute x1, starting transfers between devices, local(): got = lax.ppermute(sent, 'kv', [(i, i ^ 1) for i in range(kv)])  3.26 us
  transfers between devices with their start and end apart: 3, of which 3 were waited for; matrix products, arithmetic and copies ran while one was open for 0% of the time, Pallas kernels for 0%

profile of v8, /device:TPU:1, one launch (start us, length us, event | category | flops | bytes accessed | tf_op | source)
XLA Modules:
  0.0 126.1 jit_solution(4237879943107858833)
XLA Ops:
  0.6 1.8 %project.1 = (bf16[128,1920]{1,0:T(8,128)(2,1)S(1)}, f32[1,256]{1,0:T(1,128)S(1)}, bf16[4,128]{1,0:T(4,128)(2,1)S(1)}, bf16[1,64]{1,0:T(2,128)(2,1)S(1)}) custom-call(bf16[64,128]{1,0:T(8,128)(2,1)} %bitcast.15, bf16[1,64]{1,0:T(2,128)(2,1)} %bitcast.19, bf16[64,256]{1,0:T(8,128)(2,1)} %refs_2_.1, bf16[64,256]{1,0:T(8,128)(2,1)} %refs_3_.1, ...), custom_call_target="tpu_custom_call" | custom-call | tf_op jit(solution)/shard_map/project/pallas_call | solution.py:79
  2.4 0.0 copy-start
  2.4 0.2 reshape.37
  2.6 33.8 %all_to_all.30 = bf16[64,2,1920]{2,1,0:T(2,128)(2,1)S(1)} all-to-all(bf16[64,2,1920]{2,1,0:T(2,128)(2,1)S(1)} %reshape.37), channel_id=1, replica_groups=mesh['kv'=64,'tp'=8] {'kv'}, dimensions={0} | all-to-all | bytes 983040 | tf_op jit(solution)/shard_map/all_to_all | solution.py:304
  36.4 0.4 convert_reduce_fusion.sums
  36.9 0.0 copy-done
  36.9 0.5 attend.1
  37.3 0.7 broadcast_in_dim.21
  38.1 6.5 %all-to-all-start.1 = ((bf16[64,2,512]{2,1,0:T(2,128)(2,1)}), bf16[64,2,512]{2,1,0:T(2,128)(2,1)S(1)}, u32[]{:S(2)}, u32[]{:S(2)}) async-start(bf16[64,2,512]{2,1,0:T(2,128)(2,1)} %broadcast_in_dim.21), calls=%async_computation.1 | async-start | bytes 262144 | tf_op jit(solution)/shard_map/all_to_all | solution.py:304
  44.6 0.2 multiply_add_fusion._
  44.8 0.0 copy-start.1
  44.8 0.0 copy-start.5
  44.8 11.3 %all-to-all-done.1 = bf16[64,2,512]{2,1,0:T(2,128)(2,1)S(1)} async-done(((bf16[64,2,512]{2,1,0:T(2,128)(2,1)}), bf16[64,2,512]{2,1,0:T(2,128)(2,1)S(1)}, u32[]{:S(2)}, u32[]{:S(2)}) %all-to-all-start.1) | async-done | bytes 131104 | tf_op jit(solution)/shard_map/all_to_all | solution.py:304
  56.1 0.1 reshape.38.heads
  56.2 0.0 copy-done.5
  56.2 0.0 copy-start.4
  56.2 0.9 join.1
  57.1 0.0 copy-start.2
  57.1 0.0 copy-start.3
  57.1 0.0 copy-start.6
  57.1 7.5 %all-to-all-start.2 = ((bf16[16,64,128]{2,1,0:T(8,128)(2,1)}), bf16[16,64,128]{2,1,0:T(8,128)(2,1)S(1)}, u32[]{:S(2)}, u32[]{:S(2)}) async-start(bf16[16,64,128]{2,1,0:T(8,128)(2,1)} %join.1), calls=%async_computation.2 | async-start | bytes 524288 | tf_op jit(solution)/shard_map/all_to_all | solution.py:304
  64.6 0.0 copy-done.4
  64.6 0.0 copy-done.2
  64.7 0.0 copy-done.3
  64.7 0.0 copy-done.6
  64.7 0.2 pack.1
  64.8 3.3 %collective-permute-start = (bf16[64,2432]{1,0:T(8,128)(2,1)S(1)}, bf16[64,2432]{1,0:T(8,128)(2,1)S(1)}, u32[]{:S(2)}, u32[]{:S(2)}) collective-permute-start(bf16[64,2432]{1,0:T(8,128)(2,1)S(1)} %get-tuple-element.26), channel_id=1, source_target_pairs={{0,8},{8,0},{16,24},{24,16},{32,40},{40,32},{48,56},{56,48},{64,72... | collective-permute-start | bytes 933896 | tf_op jit(solution)/shard_map/ppermute | solution.py:345
  68.1 3.8 %all-to-all-done.2 = bf16[16,64,128]{2,1,0:T(8,128)(2,1)S(1)} async-done(((bf16[16,64,128]{2,1,0:T(8,128)(2,1)}), bf16[16,64,128]{2,1,0:T(8,128)(2,1)S(1)}, u32[]{:S(2)}, u32[]{:S(2)}) %all-to-all-start.2) | async-done | bytes 262176 | tf_op jit(solution)/shard_map/all_to_all | solution.py:304
  71.9 4.4 %collective-permute-done.got = bf16[64,2432]{1,0:T(8,128)(2,1)S(1)} collective-permute-done((bf16[64,2432]{1,0:T(8,128)(2,1)S(1)}, bf16[64,2432]{1,0:T(8,128)(2,1)S(1)}, u32[]{:S(2)}, u32[]{:S(2)}) %collective-permute-start) | collective-permute-done | bytes 311328 | tf_op jit(solution)/shard_map/ppermute | solution.py:345
  76.3 0.0 copy-done.1
  76.3 0.3 widen.1
  76.7 17.3 %all_to_all.31 = bf16[32,4,1408]{2,1,0:T(4,128)(2,1)S(1)} all-to-all(bf16[32,4,1408]{2,1,0:T(4,128)(2,1)S(1)} %get-tuple-element.29), channel_id=1, replica_groups={{0,16,40,56,64,80,104,120,128,144,168,184,192,208,232,248,256,272,296,3..., dimensions={0} | all-to-all | bytes 720896 | tf_op jit(solution)/shard_map/all_to_all | solution.py:304
  93.9 0.2 convert_reduce_fusion.1.sums
  94.1 0.2 gate.1
  94.3 15.5 %all_to_all.32 = bf16[32,4,768]{2,1,0:T(4,128)(2,1)S(1)} all-to-all(bf16[32,4,768]{2,1,0:T(4,128)(2,1)S(1)} %gate.1), channel_id=1, replica_groups={{0,16,40,56,64,80,104,120,128,144,168,184,192,208,232,248,256,272,296,3..., dimensions={0} | all-to-all | bytes 393216 | tf_op jit(solution)/shard_map/all_to_all | solution.py:304
  109.8 0.1 reshape.40.hidden
  109.8 0.2 narrow.1
  110.1 15.4 %all_to_all.33 = bf16[16,64,128]{2,1,0:T(8,128)(2,1)S(1)} all-to-all(bf16[16,64,128]{2,1,0:T(8,128)(2,1)S(1)} %bitcast.12), channel_id=1, replica_groups={{0,1,2,3,4,5,6,7,8,9,10,11,12,13,14,15},{16,17,18,19,20,21,22,23,24,25,..., dimensions={0} | all-to-all | bytes 524288 | tf_op jit(solution)/shard_map/all_to_all | solution.py:304
  125.5 0.6 fusion
  (2 shorter events, 0.1 us)
Async XLA Ops:
  2.4 34.4 %copy-start = (f32[2,1,256,512]{3,2,1,0:T(8,128)S(1)}, f32[2,1,256,512]{3,2,1,0:T(8,128)}, u32[]{:S(2)}) copy-start(f32[2,1,256,512]{3,2,1,0:T(8,128)} %state.1) | copy-start | bytes 3145732
  38.1 18.0 %all-to-all-start.1 = ((bf16[64,2,512]{2,1,0:T(2,128)(2,1)}), bf16[64,2,512]{2,1,0:T(2,128)(2,1)S(1)}, u32[]{:S(2)}, u32[]{:S(2)}) async-start(bf16[64,2,512]{2,1,0:T(2,128)(2,1)} %broadcast_in_dim.21), calls=%async_computation.1 | async-start | bytes 262144 | tf_op jit(solution)/shard_map/all_to_all | solution.py:304
  44.8 31.6 %copy-start.1 = (f32[2,1,256,512]{3,2,1,0:T(8,128)}, f32[2,1,256,512]{3,2,1,0:T(8,128)S(1)}, u32[]{:S(2)}) copy-start(f32[2,1,256,512]{3,2,1,0:T(8,128)S(1)} %multiply_add_fusion._) | copy-start | bytes 3145732
  44.8 11.4 %copy-start.5 = (bf16[512,64]{0,1:T(8,128)(2,1)S(1)}, bf16[512,64]{0,1:T(8,128)(2,1)}, u32[]{:S(2)}) copy-start(bf16[512,64]{0,1:T(8,128)(2,1)} %param.25) | copy-start | bytes 196612
  56.2 8.4 %copy-start.4 = (bf16[1376,64]{0,1:T(8,128)(2,1)S(1)}, bf16[1376,64]{0,1:T(8,128)(2,1)}, u32[]{:S(2)}) copy-start(bf16[1376,64]{0,1:T(8,128)(2,1)} %param.28) | copy-start | bytes 528388
  57.1 7.6 %copy-start.2 = (bf16[64,1376]{1,0:T(8,128)(2,1)S(1)}, bf16[64,1376]{1,0:T(8,128)(2,1)}, u32[]{:S(2)}) copy-start(bf16[64,1376]{1,0:T(8,128)(2,1)} %refs_0_.1) | copy-start | bytes 528388
  57.1 7.6 %copy-start.3 = (bf16[64,1376]{1,0:T(8,128)(2,1)S(1)}, bf16[64,1376]{1,0:T(8,128)(2,1)}, u32[]{:S(2)}) copy-start(bf16[64,1376]{1,0:T(8,128)(2,1)} %refs_1_.1) | copy-start | bytes 528388
  57.1 7.6 %copy-start.6 = (bf16[128,64]{0,1:T(8,128)(2,1)S(1)}, bf16[128,64]{0,1:T(8,128)(2,1)}, u32[]{:S(2)}) copy-start(bf16[128,64]{0,1:T(8,128)(2,1)} %param.15) | copy-start | bytes 49156
  57.1 14.8 %all-to-all-start.2 = ((bf16[16,64,128]{2,1,0:T(8,128)(2,1)}), bf16[16,64,128]{2,1,0:T(8,128)(2,1)S(1)}, u32[]{:S(2)}, u32[]{:S(2)}) async-start(bf16[16,64,128]{2,1,0:T(8,128)(2,1)} %join.1), calls=%async_computation.2 | async-start | bytes 524288 | tf_op jit(solution)/shard_map/all_to_all | solution.py:304
  64.8 11.5 %collective-permute-start = (bf16[64,2432]{1,0:T(8,128)(2,1)S(1)}, bf16[64,2432]{1,0:T(8,128)(2,1)S(1)}, u32[]{:S(2)}, u32[]{:S(2)}) collective-permute-start(bf16[64,2432]{1,0:T(8,128)(2,1)S(1)} %get-tuple-element.26), channel_id=1, source_target_pairs={{0,8},{8,0},{16,24},{24,16},{32,40},{40,32},{48,56},{56,48},{64,72... | collective-permute-start | bytes 933896 | tf_op jit(solution)/shard_map/ppermute | solution.py:345

commit v9 on v8

--- a/solution.py
+++ b/solution.py
@@ -10,8 +10,12 @@
 epsilon = 1e-06
 
 
+STRIDE = 8
+
+
 def member(kv):
-    return (kv ^ (kv >> 2)) & 1
+    place = kv // STRIDE
+    return (place ^ (place >> 2)) & 1
 
 
 def lines(kv):
@@ -20,8 +24,9 @@
 
 def pairs(kv, tp):
     return [
-        [i * tp + t for i in sorted((j, j + 1), key=member) for t in range(tp)]
-        for j in range(0, kv, 2)
+        [i * tp + t for i in sorted((j, j ^ STRIDE), key=member) for t in range(tp)]
+        for j in range(kv)
+        if j < j ^ STRIDE
     ]
 
 
@@ -342,7 +347,7 @@
     keys, values, decay, head_out = attend(summed(arrived), bias, head_scale, state, model_width)
     heads_all = exchanged(copies_of(head_out, kv), "kv")
     mine, sent = pack(head_out, tokens.T, ffn_scale, (w_ffgate, w_ffup, w_down.T))
-    got = lax.ppermute(sent, "kv", [(i, i ^ 1) for i in range(kv)])
+    got = lax.ppermute(sent, "kv", [(i, i ^ STRIDE) for i in range(kv)])
     new_state = (
         decay[:, None, :, None] * state + keys[:, None, :, None] * values[:, None, None, :]
     )

time: 127 us -> 127 us (level)
  no operation moved by 1% of the time
where the time goes in v9:
time: 127 us; the launch traced here: 126 us
  blocking collectives  82 us (65%)
  waiting for transfers between devices  19.5 us (15%)
  starting transfers between devices  17.2 us (14%)
  Pallas kernels  4.08 us (3%)
  other arithmetic  1.44 us (1%)
    all_to_all x4, blocking collectives, exchanged(): lax.all_to_all(blocks, axis, 0, 0, axis_index_groups=groups, tiled=True)  82 us
    all_to_all x2, waiting for transfers between devices, exchanged(): lax.all_to_all(blocks, axis, 0, 0, axis_index_groups=groups, tiled=True)  15.1 us
    all_to_all x2, starting transfers between devices, exchanged(): lax.all_to_all(blocks, axis, 0, 0, axis_index_groups=groups, tiled=True)  13.9 us
    ppermute x1, waiting for transfers between devices, local(): got = lax.ppermute(sent, 'kv', [(i, i ^ STRIDE) for i in range(kv)])  4.43 us
    ppermute x1, starting transfers between devices, local(): got = lax.ppermute(sent, 'kv', [(i, i ^ STRIDE) for i in range(kv)])  3.26 us
  transfers between devices with their start and end apart: 3, of which 3 were waited for; matrix products, arithmetic and copies ran while one was open for 0% of the time, Pallas kernels for 0%

profile of v9, /device:TPU:1, one launch (start us, length us, event | category | flops | bytes accessed | tf_op | source)
XLA Modules:
  0.0 126.1 jit_solution(2264163249490448944)
XLA Ops:
  0.6 1.8 %project.1 = (bf16[128,1920]{1,0:T(8,128)(2,1)S(1)}, f32[1,256]{1,0:T(1,128)S(1)}, bf16[4,128]{1,0:T(4,128)(2,1)S(1)}, bf16[1,64]{1,0:T(2,128)(2,1)S(1)}) custom-call(bf16[64,128]{1,0:T(8,128)(2,1)} %bitcast.15, bf16[1,64]{1,0:T(2,128)(2,1)} %bitcast.19, bf16[64,256]{1,0:T(8,128)(2,1)} %refs_2_.1, bf16[64,256]{1,0:T(8,128)(2,1)} %refs_3_.1, ...), custom_call_target="tpu_custom_call" | custom-call | tf_op jit(solution)/shard_map/project/pallas_call | solution.py:84
  2.4 0.0 copy-start
  2.4 0.2 reshape.37
  2.6 33.8 %all_to_all.30 = bf16[64,2,1920]{2,1,0:T(2,128)(2,1)S(1)} all-to-all(bf16[64,2,1920]{2,1,0:T(2,128)(2,1)S(1)} %reshape.37), channel_id=1, replica_groups=mesh['kv'=64,'tp'=8] {'kv'}, dimensions={0} | all-to-all | bytes 983040 | tf_op jit(solution)/shard_map/all_to_all | solution.py:309
  36.4 0.4 convert_reduce_fusion.sums
  36.9 0.0 copy-done
  36.9 0.5 attend.1
  37.3 0.7 broadcast_in_dim.21
  38.1 6.5 %all-to-all-start.1 = ((bf16[64,2,512]{2,1,0:T(2,128)(2,1)}), bf16[64,2,512]{2,1,0:T(2,128)(2,1)S(1)}, u32[]{:S(2)}, u32[]{:S(2)}) async-start(bf16[64,2,512]{2,1,0:T(2,128)(2,1)} %broadcast_in_dim.21), calls=%async_computation.1 | async-start | bytes 262144 | tf_op jit(solution)/shard_map/all_to_all | solution.py:309
  44.6 0.2 multiply_add_fusion._
  44.8 0.0 copy-start.1
  44.8 0.0 copy-start.5
  44.8 11.3 %all-to-all-done.1 = bf16[64,2,512]{2,1,0:T(2,128)(2,1)S(1)} async-done(((bf16[64,2,512]{2,1,0:T(2,128)(2,1)}), bf16[64,2,512]{2,1,0:T(2,128)(2,1)S(1)}, u32[]{:S(2)}, u32[]{:S(2)}) %all-to-all-start.1) | async-done | bytes 131104 | tf_op jit(solution)/shard_map/all_to_all | solution.py:309
  56.1 0.1 reshape.38.heads
  56.2 0.0 copy-done.5
  56.2 0.0 copy-start.4
  56.2 0.9 join.1
  57.1 0.0 copy-start.2
  57.1 0.0 copy-start.3
  57.1 0.0 copy-start.6
  57.1 7.4 %all-to-all-start.2 = ((bf16[16,64,128]{2,1,0:T(8,128)(2,1)}), bf16[16,64,128]{2,1,0:T(8,128)(2,1)S(1)}, u32[]{:S(2)}, u32[]{:S(2)}) async-start(bf16[16,64,128]{2,1,0:T(8,128)(2,1)} %join.1), calls=%async_computation.2 | async-start | bytes 524288 | tf_op jit(solution)/shard_map/all_to_all | solution.py:309
  64.5 0.0 copy-done.4
  64.5 0.0 copy-done.2
  64.5 0.0 copy-done.3
  64.6 0.0 copy-done.6
  64.6 0.2 pack.1
  64.7 3.3 %collective-permute-start = (bf16[64,2432]{1,0:T(8,128)(2,1)S(1)}, bf16[64,2432]{1,0:T(8,128)(2,1)S(1)}, u32[]{:S(2)}, u32[]{:S(2)}) collective-permute-start(bf16[64,2432]{1,0:T(8,128)(2,1)S(1)} %get-tuple-element.26), channel_id=1, source_target_pairs={{0,64},{8,72},{16,80},{24,88},{32,96},{40,104},{48,112},{56,120},{... | collective-permute-start | bytes 933896 | tf_op jit(solution)/shard_map/ppermute | solution.py:350
  68.0 3.8 %all-to-all-done.2 = bf16[16,64,128]{2,1,0:T(8,128)(2,1)S(1)} async-done(((bf16[16,64,128]{2,1,0:T(8,128)(2,1)}), bf16[16,64,128]{2,1,0:T(8,128)(2,1)S(1)}, u32[]{:S(2)}, u32[]{:S(2)}) %all-to-all-start.2) | async-done | bytes 262176 | tf_op jit(solution)/shard_map/all_to_all | solution.py:309
  71.8 4.4 %collective-permute-done.got = bf16[64,2432]{1,0:T(8,128)(2,1)S(1)} collective-permute-done((bf16[64,2432]{1,0:T(8,128)(2,1)S(1)}, bf16[64,2432]{1,0:T(8,128)(2,1)S(1)}, u32[]{:S(2)}, u32[]{:S(2)}) %collective-permute-start) | collective-permute-done | bytes 311328 | tf_op jit(solution)/shard_map/ppermute | solution.py:350
  76.2 0.0 copy-done.1
  76.2 0.3 widen.1
  76.6 15.7 %all_to_all.31 = bf16[32,4,1408]{2,1,0:T(4,128)(2,1)S(1)} all-to-all(bf16[32,4,1408]{2,1,0:T(4,128)(2,1)S(1)} %get-tuple-element.29), channel_id=1, replica_groups={{0,8,16,24,32,40,48,56,128,136,144,152,160,168,176,184,320,328,336,344,..., dimensions={0} | all-to-all | bytes 720896 | tf_op jit(solution)/shard_map/all_to_all | solution.py:309
  92.3 0.2 convert_reduce_fusion.1.sums
  92.5 0.2 gate.1
  92.7 18.2 %all_to_all.32 = bf16[32,4,768]{2,1,0:T(4,128)(2,1)S(1)} all-to-all(bf16[32,4,768]{2,1,0:T(4,128)(2,1)S(1)} %gate.1), channel_id=1, replica_groups={{0,8,16,24,32,40,48,56,128,136,144,152,160,168,176,184,320,328,336,344,..., dimensions={0} | all-to-all | bytes 393216 | tf_op jit(solution)/shard_map/all_to_all | solution.py:309
  110.9 0.1 reshape.40.hidden
  110.9 0.2 narrow.1
  111.2 14.3 %all_to_all.33 = bf16[16,64,128]{2,1,0:T(8,128)(2,1)S(1)} all-to-all(bf16[16,64,128]{2,1,0:T(8,128)(2,1)S(1)} %bitcast.12), channel_id=1, replica_groups={{0,1,2,3,4,5,6,7,64,65,66,67,68,69,70,71},{8,9,10,11,12,13,14,15,72,73,..., dimensions={0} | all-to-all | bytes 524288 | tf_op jit(solution)/shard_map/all_to_all | solution.py:309
  125.5 0.6 fusion
  (2 shorter events, 0.1 us)
Async XLA Ops:
  2.4 34.4 %copy-start = (f32[2,1,256,512]{3,2,1,0:T(8,128)S(1)}, f32[2,1,256,512]{3,2,1,0:T(8,128)}, u32[]{:S(2)}) copy-start(f32[2,1,256,512]{3,2,1,0:T(8,128)} %state.1) | copy-start | bytes 3145732
  38.1 18.0 %all-to-all-start.1 = ((bf16[64,2,512]{2,1,0:T(2,128)(2,1)}), bf16[64,2,512]{2,1,0:T(2,128)(2,1)S(1)}, u32[]{:S(2)}, u32[]{:S(2)}) async-start(bf16[64,2,512]{2,1,0:T(2,128)(2,1)} %broadcast_in_dim.21), calls=%async_computation.1 | async-start | bytes 262144 | tf_op jit(solution)/shard_map/all_to_all | solution.py:309
  44.8 31.4 %copy-start.1 = (f32[2,1,256,512]{3,2,1,0:T(8,128)}, f32[2,1,256,512]{3,2,1,0:T(8,128)S(1)}, u32[]{:S(2)}) copy-start(f32[2,1,256,512]{3,2,1,0:T(8,128)S(1)} %multiply_add_fusion._) | copy-start | bytes 3145732
  44.8 11.4 %copy-start.5 = (bf16[512,64]{0,1:T(8,128)(2,1)S(1)}, bf16[512,64]{0,1:T(8,128)(2,1)}, u32[]{:S(2)}) copy-start(bf16[512,64]{0,1:T(8,128)(2,1)} %param.25) | copy-start | bytes 196612
  56.2 8.3 %copy-start.4 = (bf16[1376,64]{0,1:T(8,128)(2,1)S(1)}, bf16[1376,64]{0,1:T(8,128)(2,1)}, u32[]{:S(2)}) copy-start(bf16[1376,64]{0,1:T(8,128)(2,1)} %param.28) | copy-start | bytes 528388
  57.1 7.4 %copy-start.2 = (bf16[64,1376]{1,0:T(8,128)(2,1)S(1)}, bf16[64,1376]{1,0:T(8,128)(2,1)}, u32[]{:S(2)}) copy-start(bf16[64,1376]{1,0:T(8,128)(2,1)} %refs_0_.1) | copy-start | bytes 528388
  57.1 7.4 %copy-start.3 = (bf16[64,1376]{1,0:T(8,128)(2,1)S(1)}, bf16[64,1376]{1,0:T(8,128)(2,1)}, u32[]{:S(2)}) copy-start(bf16[64,1376]{1,0:T(8,128)(2,1)} %refs_1_.1) | copy-start | bytes 528388
  57.1 7.5 %copy-start.6 = (bf16[128,64]{0,1:T(8,128)(2,1)S(1)}, bf16[128,64]{0,1:T(8,128)(2,1)}, u32[]{:S(2)}) copy-start(bf16[128,64]{0,1:T(8,128)(2,1)} %param.15) | copy-start | bytes 49156
  57.1 14.7 %all-to-all-start.2 = ((bf16[16,64,128]{2,1,0:T(8,128)(2,1)}), bf16[16,64,128]{2,1,0:T(8,128)(2,1)S(1)}, u32[]{:S(2)}, u32[]{:S(2)}) async-start(bf16[16,64,128]{2,1,0:T(8,128)(2,1)} %join.1), calls=%async_computation.2 | async-start | bytes 524288 | tf_op jit(solution)/shard_map/all_to_all | solution.py:309
  64.7 11.5 %collective-permute-start = (bf16[64,2432]{1,0:T(8,128)(2,1)S(1)}, bf16[64,2432]{1,0:T(8,128)(2,1)S(1)}, u32[]{:S(2)}, u32[]{:S(2)}) collective-permute-start(bf16[64,2432]{1,0:T(8,128)(2,1)S(1)} %get-tuple-element.26), channel_id=1, source_target_pairs={{0,64},{8,72},{16,80},{24,88},{32,96},{40,104},{48,112},{56,120},{... | collective-permute-start | bytes 933896 | tf_op jit(solution)/shard_map/ppermute | solution.py:350
